TPU v7x, 32 devices: a whole 2x2x4 slice. The times are simulated.
32 devices in a mesh: ep: 8 (over z, y), tp: 4 (over x, core).
Axes of the slice: x: 2, y: 2, z: 4, core: 2. Of those that a mesh axis runs over, the one named last changes fastest.
Arguments:
- tokens: bfloat16 [2560, 2048], P('ep'), may hold values from -12 to 12, as said below
- cotangent: bfloat16 [2560, 2048], P('ep'), may hold values from -0.59765625 to 0.59765625
- route_ids: int32 [2560, 2], P('ep'), may hold values from 0 to 7, all different within a row; in each aligned block of 320 rows (0 to 319, 320 to 639, ...) at most 160 rows name the same one
- route_weights: bfloat16 [2560, 2], P('ep'), may hold values from 0.049804688 to 1
- w_gate: bfloat16 [8, 2048, 2048], P('ep', None, 'tp'), may hold values from -0.125 to 0.125
- w_up: bfloat16 [8, 2048, 2048], P('ep', None, 'tp'), may hold values from -0.125 to 0.125
- w_down: bfloat16 [8, 2048, 2048], P('ep', 'tp'), may hold values from -0.125 to 0.125
- dense_in: bfloat16 [2048, 256], P(('ep', 'tp')), may hold values from -0.125 to 0.125
- dense_out: bfloat16 [2048, 256], P(('ep', 'tp')), may hold values from -0.375 to 0.375
- dense_gate: bfloat16 [2048], replicated, may hold values from -0.125 to 0.125
Outputs:
- grad_tokens: bfloat16 [2560, 2048], P('ep', 'tp')
- grad_route_weights: bfloat16 [2560, 2], P('ep')
- grad_gate: float32 [8, 2048, 2048], P('ep', None, 'tp')
- grad_up: float32 [8, 2048, 2048], P('ep', None, 'tp')
- grad_down: float32 [8, 2048, 2048], P('ep', 'tp')
- grad_dense_in: float32 [2048, 256], P(('ep', 'tp'))
- grad_dense_out: float32 [2048, 256], P(('ep', 'tp'))
- grad_dense_gate: float32 [2048], P(('ep', 'tp'))
Inputs may be any that keep to these rules, and one draw needn't show every extreme that they name: `route_ids`: each row names 2 different experts; among the rows of one index of ep no expert is named more than 160 times, and that count is reached. `tokens`: rows carry scales between 0.5 and 2 that differ from row to row.
All inputs are finite; a program needn't handle non-finite values.
Results may differ from a plain program's by a relative error of at most 0.01.
Values may be sent and summed in bfloat16 or wider, within the bound.
A program may use at most 128 MiB of HBM per device.

v0:
```python
import jax
import jax.numpy as jnp
from jax import lax
from jax.sharding import PartitionSpec as P

CLAMP_LIMIT = 7.0
SIG_SLOPE = 1.702


def shards(
    tokens,
    cotangent,
    route_ids,
    route_weights,
    w_gate,
    w_up,
    w_down,
    dense_in,
    dense_out,
    dense_gate,
):
    count_ep = lax.axis_size("ep")
    count_tp = lax.axis_size("tp")
    tp_index = lax.axis_index("tp")
    tok_dev, model_width = tokens.shape
    top_k = route_ids.shape[1]
    col_count = model_width // count_tp
    capacity = 2 * tok_dev * top_k // count_ep
    assigns = tok_dev * top_k
    slot_total = count_ep * capacity
    flat_ids = route_ids.reshape(-1)
    one_hot = (flat_ids[:, None] == jnp.arange(count_ep, dtype=jnp.int32)[None, :]).astype(
        jnp.int32
    )
    earlier = jnp.cumsum(one_hot, axis=0) - one_hot
    slot_index = jnp.sum(earlier * one_hot, axis=1)
    target = flat_ids * capacity + slot_index
    matches = target[None, :] == jnp.arange(slot_total, dtype=jnp.int32)[:, None]
    filled = jnp.any(matches, axis=1)
    source = jnp.sum(jnp.where(matches, jnp.arange(assigns, dtype=jnp.int32)[None, :], 0), axis=1)
    token_of = source // top_k
    x_rows = jnp.where(filled[:, None], tokens[token_of], jnp.zeros((), jnp.bfloat16)).reshape(
        count_ep, capacity, model_width
    )
    dy_rows = jnp.where(filled[:, None], cotangent[token_of], jnp.zeros((), jnp.bfloat16)).reshape(
        count_ep, capacity, model_width
    )
    weight_rows = jnp.where(
        filled, route_weights.reshape(-1)[source], jnp.zeros((), jnp.bfloat16)
    ).reshape(count_ep, capacity)
    x_part = lax.dynamic_slice_in_dim(x_rows, tp_index * col_count, col_count, 2)
    dy_part = lax.dynamic_slice_in_dim(dy_rows, tp_index * col_count, col_count, 2)
    x_quarter, dy_quarter, weight_in = (
        lax.all_to_all(x_part, "ep", split_axis=0, concat_axis=0, tiled=True),
        lax.all_to_all(dy_part, "ep", split_axis=0, concat_axis=0, tiled=True),
        lax.all_to_all(weight_rows, "ep", split_axis=0, concat_axis=0, tiled=True),
    )
    x_in, dy_in = (
        lax.all_gather(x_quarter, "tp", axis=2, tiled=True),
        lax.all_gather(dy_quarter, "tp", axis=2, tiled=True),
    )
    x_slots = x_in.reshape(slot_total, model_width)
    dy_slots = dy_in.reshape(slot_total, model_width)
    route_col = weight_in.reshape(slot_total, 1).astype(jnp.float32)
    gate_w = w_gate[0]
    up_w = w_up[0]
    down_w = w_down[0]
    gate_pre = jnp.dot(x_slots, gate_w, preferred_element_type=jnp.float32)
    up_pre = jnp.dot(x_slots, up_w, preferred_element_type=jnp.float32)
    gate_clamp = jnp.minimum(gate_pre, CLAMP_LIMIT)
    up_clamp = jnp.clip(up_pre, -CLAMP_LIMIT, CLAMP_LIMIT)
    sig = jax.nn.sigmoid(SIG_SLOPE * gate_clamp)
    act = (gate_clamp * sig * (up_clamp + 1.0)).astype(jnp.bfloat16)
    back = lax.dot_general(
        dy_slots, down_w, (((1,), (1,)), ((), ())), preferred_element_type=jnp.float32
    )
    d_act = route_col * back
    d_gate = jnp.where(
        gate_pre < CLAMP_LIMIT,
        d_act * (up_clamp + 1.0) * (sig + SIG_SLOPE * gate_clamp * sig * (1.0 - sig)),
        0.0,
    ).astype(jnp.bfloat16)
    d_up = jnp.where(jnp.abs(up_pre) < CLAMP_LIMIT, d_act * gate_clamp * sig, 0.0).astype(
        jnp.bfloat16
    )
    scaled_cot = (route_col * dy_slots.astype(jnp.float32)).astype(jnp.bfloat16)
    contract_rows = (((0,), (0,)), ((), ()))
    grad_gate = lax.dot_general(x_slots, d_gate, contract_rows, preferred_element_type=jnp.float32)
    grad_up = lax.dot_general(x_slots, d_up, contract_rows, preferred_element_type=jnp.float32)
    grad_down = lax.dot_general(act, scaled_cot, contract_rows, preferred_element_type=jnp.float32)
    contract_cols = (((1,), (1,)), ((), ()))
    row_partial = lax.dot_general(d_gate, gate_w, contract_cols, preferred_element_type=jnp.float32)
    row_partial = row_partial + lax.dot_general(
        d_up, up_w, contract_cols, preferred_element_type=jnp.float32
    )
    row_cols = lax.psum_scatter(
        row_partial.reshape(count_ep, capacity, model_width).astype(jnp.bfloat16),
        "tp",
        scatter_dimension=2,
        tiled=True,
    )
    weight_grad = lax.psum(jnp.sum(act.astype(jnp.float32) * back, axis=1), "tp").astype(
        jnp.bfloat16
    )
    back_rows, back_weights = (
        lax.all_to_all(row_cols, "ep", split_axis=0, concat_axis=0, tiled=True),
        lax.all_to_all(
            weight_grad.reshape(count_ep, capacity), "ep", split_axis=0, concat_axis=0, tiled=True
        ),
    )
    expert_dx = (
        back_rows.reshape(slot_total, col_count)[target]
        .astype(jnp.float32)
        .reshape(tok_dev, top_k, col_count)
    )
    expert_dx = jnp.sum(expert_dx, axis=1)
    grad_route_weights = back_weights.reshape(-1)[target].reshape(tok_dev, top_k)
    in_whole, out_whole = (
        lax.all_gather(dense_in, ("ep", "tp"), axis=0, tiled=True),
        lax.all_gather(dense_out, ("ep", "tp"), axis=0, tiled=True),
    )
    dense_pre = jnp.dot(tokens, in_whole, preferred_element_type=jnp.float32)
    dense_act = jax.nn.silu(dense_pre).astype(jnp.bfloat16)
    dense_val = lax.dot_general(
        dense_act, out_whole, contract_cols, preferred_element_type=jnp.float32
    )
    mix = jax.nn.sigmoid(jnp.dot(tokens, dense_gate, preferred_element_type=jnp.float32))
    cot_wide = cotangent.astype(jnp.float32)
    dense_scaled = (mix[:, None] * cot_wide).astype(jnp.bfloat16)
    dense_back = jnp.dot(dense_scaled, out_whole, preferred_element_type=jnp.float32)
    sig_pre = jax.nn.sigmoid(dense_pre)
    dense_dpre = (dense_back * sig_pre * (1.0 + dense_pre * (1.0 - sig_pre))).astype(jnp.bfloat16)
    dlogit = mix * (1.0 - mix) * jnp.sum(cot_wide * dense_val, axis=1)
    in_rows = lax.dynamic_slice_in_dim(in_whole, tp_index * col_count, col_count, 0)
    gate_cols = lax.dynamic_slice_in_dim(dense_gate, tp_index * col_count, col_count, 0)
    dense_dx = lax.dot_general(
        dense_dpre, in_rows, contract_cols, preferred_element_type=jnp.float32
    )
    dense_dx = dense_dx + dlogit[:, None] * gate_cols.astype(jnp.float32)[None, :]
    grad_tokens = (dense_dx + expert_dx).astype(jnp.bfloat16)
    block_cols = model_width // (count_ep * count_tp)
    tokens_own = lax.dynamic_index_in_dim(
        tokens.reshape(tok_dev, count_ep, count_tp, block_cols), tp_index, 2, keepdims=False
    ).reshape(tok_dev, count_ep * block_cols)
    scaled_own = lax.dynamic_index_in_dim(
        dense_scaled.reshape(tok_dev, count_ep, count_tp, block_cols), tp_index, 2, keepdims=False
    ).reshape(tok_dev, count_ep * block_cols)
    in_partial = lax.dot_general(
        tokens_own, dense_dpre, contract_rows, preferred_element_type=jnp.float32
    )
    out_partial = lax.dot_general(
        scaled_own, dense_act, contract_rows, preferred_element_type=jnp.float32
    )
    gate_partial = jnp.sum(tokens_own.astype(jnp.float32) * dlogit[:, None], axis=0)
    grad_dense_in, grad_dense_out, grad_dense_gate = (
        lax.psum_scatter(in_partial, "ep", scatter_dimension=0, tiled=True),
        lax.psum_scatter(out_partial, "ep", scatter_dimension=0, tiled=True),
        lax.psum_scatter(gate_partial, "ep", scatter_dimension=0, tiled=True),
    )
    return (
        grad_tokens,
        grad_route_weights,
        grad_gate[None],
        grad_up[None],
        grad_down[None],
        grad_dense_in,
        grad_dense_out,
        grad_dense_gate,
    )


def solution(mesh):
    placed = (
        P("ep", None),
        P("ep", None),
        P("ep", None),
        P("ep", None),
        P("ep", None, "tp"),
        P("ep", None, "tp"),
        P("ep", "tp", None),
        P(("ep", "tp"), None),
        P(("ep", "tp"), None),
        P(),
    )
    return jax.shard_map(
        shards,
        mesh=mesh,
        in_specs=placed,
        out_specs=(
            P("ep", "tp"),
            P("ep", None),
            P("ep", None, "tp"),
            P("ep", None, "tp"),
            P("ep", "tp", None),
            P(("ep", "tp"), None),
            P(("ep", "tp"), None),
            P(("ep", "tp")),
        ),
        check_vma=False,
    )
```

profile of v0, /device:TPU:13, one launch (start us, length us, event | category | flops | bytes accessed | tf_op | source)
XLA Modules:
  0.0 459.5 jit_solution(5614435239581886446)
XLA Ops:
  7.2 1.0 copy.40
  8.5 1.4 reduce-window.6
  11.4 12.4 %gather_fusion = bf16[1280,2048]{1,0:T(8,128)(2,1)} fusion(bf16[320,2048]{1,0:T(8,128)(2,1)} %param.10, s32[2048]{0:T(1024)S(1)} %get-tuple-element.47), kind=kCustom, calls=%fused_computation | custom fusion | bytes 10490880 | tf_op jit(solution)/shard_map/gather | solution.py:42
  23.8 6.1 %gather_fusion.2 = bf16[1280,2048]{1,0:T(8,128)(2,1)} fusion(bf16[320,2048]{1,0:T(8,128)(2,1)S(1)} %copy-done.3, s32[2048]{0:T(1024)S(1)} %get-tuple-element.47), kind=kCustom, calls=%fused_computation.2 | custom fusion | bytes 10490880 | tf_op jit(solution)/shard_map/gather | solution.py:45
  30.0 3.3 dynamic-slice_select_fusion
  33.3 33.9 %all_to_all.31 = bf16[8,160,512]{2,1,0:T(8,128)(2,1)} all-to-all(bf16[8,160,512]{2,1,0:T(8,128)(2,1)S(1)} %get-tuple-element.45), channel_id=1, replica_groups=mesh['ep'=8,'tp'=4] {'ep'}, dimensions={0} | all-to-all | bytes 2621440 | tf_op jit(solution)/shard_map/all_to_all | solution.py:54
  67.3 34.5 %all_to_all.32 = bf16[8,160,512]{2,1,0:T(8,128)(2,1)} all-to-all(bf16[8,160,512]{2,1,0:T(8,128)(2,1)} %get-tuple-element.44), channel_id=1, replica_groups=mesh['ep'=8,'tp'=4] {'ep'}, dimensions={0} | all-to-all | bytes 2621440 | tf_op jit(solution)/shard_map/all_to_all | solution.py:55
  101.9 0.7 all-gather.7.cloned.1.call-update
  102.9 8.0 %gather_fusion.1 = bf16[1280]{0:T(1024)(128)(2,1)S(1)} fusion(bf16[640]{0:T(1024)(128)(2,1)S(1)} %reshape.245, s32[2048]{0:T(1024)S(1)} %get-tuple-element.46), kind=kCustom, calls=%fused_computation.1 | custom fusion | bytes 10240 | tf_op jit(solution)/shard_map/gather | solution.py:49
  110.9 0.7 select_n.103
  111.6 6.5 %all-to-all-start.1 = ((bf16[8,1,160]{2,1,0:T(2,128)(2,1)}), bf16[8,1,160]{2,1,0:T(2,128)(2,1)S(1)}, u32[]{:S(2)}, u32[]{:S(2)}) async-start(bf16[8,1,160]{2,1,0:T(2,128)(2,1)} %select_n.103), calls=%async_computation.1 | async-start | bytes 16384 | tf_op jit(solution)/shard_map/all_to_all | solution.py:56
  118.0 0.6 all-gather.5.cloned.1.call-update
  118.8 2.5 all-to-all-done.1
  121.5 7.3 %fusion.12 = f32[1280,512]{0,1:T(8,128)} fusion(bf16[1280,2048]{1,0:T(8,128)(2,1)} %bitcast.73, bf16[1,2048,512]{2,1,0:T(8,128)(2,1)S(1)} %copy-done), kind=kOutput, calls=%fused_computation.32 | convolution fusion | flops 2684354560 | bytes 9961472 | tf_op jit(solution)/shard_map/dot_general | solution.py:68
  128.7 4.6 %fusion.6 = f32[1280,512]{0,1:T(8,128)} fusion(bf16[1280,2048]{1,0:T(8,128)(2,1)S(1)} %bitcast.76, bf16[1,2048,512]{2,1,0:T(8,128)(2,1)S(1)} %copy-done.9), kind=kOutput, calls=%fused_computation.26 | convolution fusion | flops 2684354560 | bytes 9961472 | tf_op jit(solution)/shard_map/dot_general | solution.py:69
  133.4 18.9 %all-gather.11.cloned.1.call-done = bf16[8,160,2048]{2,1,0:T(8,128)(2,1)} async-done(((bf16[8,160,512]{2,1,0:T(8,128)(2,1)}), bf16[8,160,2048]{2,1,0:T(8,128)(2,1)}) %all-gather.11.cloned.1.call-update) | async-done | bytes 5242896 | tf_op jit(solution)/shard_map/all_gather | solution.py:60
  152.3 10.5 %multiply_reduce_fusion = (f32[1280]{0:T(1024)S(1)}, bf16[1280,512]{0,1:T(8,128)(2,1)}, bf16[1280,512]{0,1:T(8,128)(2,1)S(1)}, bf16[1280,512]{0,1:T(8,128)(2,1)S(1)}) fusion(f32[1280,512]{0,1:T(8,128)} %fusion.6, f32[1280,512]{0,1:T(8,128)} %fusion.12, f32[1280]{0:T(1024)S(1)} %reshape.254, bf16[1280,2048]{1,0:T(8,128)(2,1)} %bitcast.77, ...), kind=kOutput, calls=%fused_computation.18 | convolution fusion | flops 2703358720 | bytes 16525312 | tf_op jit(solution)/shard_map/dot_general | solution.py:74
  162.8 3.2 fusion.10
  166.1 4.7 %add_convert_fusion = bf16[1280,2048]{1,0:T(8,128)(2,1)} fusion(f32[1280,2048]{1,0:T(8,128)S(1)} %fusion.10, bf16[1280,512]{0,1:T(8,128)(2,1)S(1)} %get-tuple-element.41, bf16[1,2048,512]{2,1,0:T(8,128)(2,1)S(1)} %copy-done.10), kind=kOutput, calls=%fused_computation.6 | convolution fusion | flops 2689597440 | bytes 19136512 | tf_op jit(solution)/shard_map/dot_general | solution.py:93
  170.9 1.2 copy-done.2
  172.1 1.5 copy.48
  174.2 33.9 %all-gather.7.cloned.1.call-done = bf16[2048,256]{1,0:T(8,128)(2,1)} async-done(((bf16[64,256]{1,0:T(8,128)(2,1)}), bf16[2048,256]{1,0:T(8,128)(2,1)}) %all-gather.7.cloned.1.call-update) | async-done | bytes 1048592 | tf_op jit(solution)/shard_map/all_gather | solution.py:119
  208.1 1.7 fusion.29
  209.8 53.6 %all-gather.5.cloned.1.call-done = bf16[2048,256]{1,0:T(8,128)(2,1)} async-done(((bf16[64,256]{1,0:T(8,128)(2,1)}), bf16[2048,256]{1,0:T(8,128)(2,1)}) %all-gather.5.cloned.1.call-update) | async-done | bytes 1048592 | tf_op jit(solution)/shard_map/all_gather | solution.py:120
  263.4 1.9 fusion.14
  265.3 1.3 multiply_reduce_fusion.1
  267.4 1.1 fusion.30
  268.9 0.6 dynamic-slice
  270.3 0.8 copy.49
  271.1 5.5 %psum.7 = bf16[1280]{0:T(1024)(128)(2,1)S(1)} all-reduce(f32[1280]{0:T(1024)S(1)} %get-tuple-element.36), channel_id=1, replica_groups=mesh['ep'=8,'tp'=4] {'tp'}, use_global_device_ids=true, to_apply=%region_9.10 | all-reduce | flops 1280 | bytes 7680 | tf_op jit(solution)/shard_map/psum | solution.py:102
  276.6 0.7 all_to_all.25
  277.3 5.2 %all-to-all-start.4 = ((bf16[8,1,160]{2,1,0:T(2,128)(2,1)}), bf16[8,1,160]{2,1,0:T(2,128)(2,1)S(1)}, u32[]{:S(2)}, u32[]{:S(2)}) async-start(bf16[8,1,160]{2,1,0:T(2,128)(2,1)} %all_to_all.25), calls=%async_computation.5 | async-start | bytes 16384 | tf_op jit(solution)/shard_map/all_to_all | solution.py:107
  282.6 3.2 all-to-all-done.4
  285.8 30.3 %reduce-scatter.4.cloned.1.call-done = bf16[8,160,512]{2,1,0:T(8,128)(2,1)} async-done(((bf16[8,160,2048]{2,1,0:T(8,128)(2,1)}), bf16[8,160,512]{2,1,0:T(8,128)(2,1)}) %reduce-scatter.4.cloned.1.call-update) | async-done | bytes 1310736 | tf_op jit(solution)/shard_map/reduce_scatter | solution.py:96
  316.1 5.5 %all-to-all-start.3 = ((bf16[8,160,512]{2,1,0:T(8,128)(2,1)}), bf16[8,160,512]{2,1,0:T(8,128)(2,1)S(1)}, u32[]{:S(2)}, u32[]{:S(2)}) async-start(bf16[8,160,512]{2,1,0:T(8,128)(2,1)} %reduce-scatter.4.cloned.1.call-done), calls=%async_computation.4 | async-start | bytes 2621440 | tf_op jit(solution)/shard_map/all_to_all | solution.py:106
  321.6 1.2 fusion.28
  322.9 38.9 %all-reduce = f32[512]{0:T(512)S(1)} all-reduce(f32[512]{0:T(512)S(1)} %reduce_sum.68), channel_id=5, replica_groups=mesh['ep'=8,'tp'=4] {'ep'}, use_global_device_ids=true, to_apply=%region_13.14.clone | all-reduce | flops 512 | bytes 4096
  361.8 0.6 dynamic-slice.1
  362.4 7.3 %convolution_bitcast_fusion = f32[1,2048,512]{2,1,0:T(8,128)} fusion(bf16[1280,2048]{1,0:T(8,128)(2,1)} %bitcast.74, bf16[1280,512]{0,1:T(8,128)(2,1)S(1)} %copy-done.19), kind=kOutput, calls=%fused_computation.15 | convolution fusion | flops 2684354560 | bytes 10747904 | tf_op jit(solution)/shard_map/dot_general | solution.py:89
  369.6 7.2 %convolution_bitcast_fusion.1 = f32[1,2048,512]{2,1,0:T(8,128)} fusion(bf16[1280,2048]{1,0:T(8,128)(2,1)} %bitcast.75, bf16[1280,512]{0,1:T(8,128)(2,1)S(1)} %copy-done.17), kind=kOutput, calls=%fused_computation.16 | convolution fusion | flops 2684354560 | bytes 10747904 | tf_op jit(solution)/shard_map/dot_general | solution.py:88
  376.9 4.6 %fusion.3 = f32[1,512,2048]{2,1,0:T(8,128)} fusion(bf16[1280,512]{0,1:T(8,128)(2,1)S(1)} %copy-done.20, bf16[1280,2048]{1,0:T(8,128)(2,1)S(1)} %bitcast.80, f32[1280]{0:T(1024)S(1)} %reshape.254), kind=kOutput, calls=%fused_computation.14 | convolution fusion | flops 2692218880 | bytes 10753024 | tf_op jit(solution)/shard_map/dot_general | solution.py:90
  381.6 4.3 gather_fusion.4
  386.1 0.7 copy.50
  386.8 3.3 gather_fusion.3
  390.1 2.0 reshape.255
  392.1 2.5 reduce_sum.65
  394.6 2.2 fusion.16
  396.8 55.9 %reduce-scatter.8.cloned.1.call-done = f32[64,256]{1,0:T(8,128)} async-done(((f32[512,256]{1,0:T(8,128)}), f32[64,256]{1,0:T(8,128)}) %reduce-scatter.8.cloned.1.call-update) | async-done | bytes 65552 | tf_op jit(solution)/shard_map/reduce_scatter | solution.py:157
  (96 shorter events, 4.9 us)
Async XLA Ops:
  7.2 114.3 %copy-start = (bf16[1,2048,512]{2,1,0:T(8,128)(2,1)S(1)}, bf16[1,2048,512]{2,1,0:T(8,128)(2,1)}, u32[]{:S(2)}) copy-start(bf16[1,2048,512]{2,1,0:T(8,128)(2,1)} %param.14) | copy-start | bytes 6291460
  7.2 114.3 %all-gather.9.cloned.1.call-start = ((), (), s32[]{:S(2)}) async-start(), calls=%async_computation.10 | async-start | bytes 6553600 | tf_op jit(solution)/shard_map/all_gather | solution.py:59
  11.4 12.4 %copy-start.3 = (bf16[320,2048]{1,0:T(8,128)(2,1)S(1)}, bf16[320,2048]{1,0:T(8,128)(2,1)}, u32[]{:S(2)}) copy-start(bf16[320,2048]{1,0:T(8,128)(2,1)} %param.11) | copy-start | bytes 3932164
  67.2 35.4 %copy-start.7 = (bf16[320,2]{0,1:T(2,128)(2,1)S(1)}, bf16[320,2]{0,1:T(2,128)(2,1)}, u32[]{:S(2)}) copy-start(bf16[320,2]{0,1:T(2,128)(2,1)} %param.13) | copy-start | bytes 3844
  67.2 85.1 %all-gather.11.cloned.1.call-start = ((), (), s32[]{:S(2)}) async-start(), calls=%async_computation.11 | async-start | bytes 6553600 | tf_op jit(solution)/shard_map/all_gather | solution.py:60
  101.8 106.2 %all-gather.7.cloned.1.call-start = ((), (), s32[]{:S(2)}) async-start(), calls=%async_computation.9 | async-start | bytes 1081344 | tf_op jit(solution)/shard_map/all_gather | solution.py:119
  111.6 9.8 %all-to-all-start.1 = ((bf16[8,1,160]{2,1,0:T(2,128)(2,1)}), bf16[8,1,160]{2,1,0:T(2,128)(2,1)S(1)}, u32[]{:S(2)}, u32[]{:S(2)}) async-start(bf16[8,1,160]{2,1,0:T(2,128)(2,1)} %select_n.103), calls=%async_computation.1 | async-start | bytes 16384 | tf_op jit(solution)/shard_map/all_to_all | solution.py:56
  118.0 145.4 %all-gather.5.cloned.1.call-start = ((), (), s32[]{:S(2)}) async-start(), calls=%async_computation.8 | async-start | bytes 1081344 | tf_op jit(solution)/shard_map/all_gather | solution.py:120
  118.6 197.5 %reduce-scatter.4.cloned.1.call-start = ((), (), s32[]{:S(2)}) async-start(), calls=%async_computation.12 | async-start | bytes 6553600 | tf_op jit(solution)/shard_map/reduce_scatter | solution.py:96
  121.4 7.3 %copy-start.8 = (bf16[8,160,2048]{2,1,0:T(8,128)(2,1)S(1)}, bf16[8,160,2048]{2,1,0:T(8,128)(2,1)}, u32[]{:S(2)}) copy-start(bf16[8,160,2048]{2,1,0:T(8,128)(2,1)} %all-gather.9.cloned.1.call-done) | copy-start | bytes 15728644
  121.5 7.3 %copy-start.9 = (bf16[1,2048,512]{2,1,0:T(8,128)(2,1)S(1)}, bf16[1,2048,512]{2,1,0:T(8,128)(2,1)}, u32[]{:S(2)}) copy-start(bf16[1,2048,512]{2,1,0:T(8,128)(2,1)} %param.15) | copy-start | bytes 6291460
  162.8 3.2 copy-start.16
  162.8 3.2 copy-start.18
  162.8 3.2 copy-start.10
  170.8 1.3 copy-start.2
  170.8 2.8 copy-start.6
  170.8 226.0 %reduce-scatter.6.cloned.1.call-start = ((), (), s32[]{:S(2)}) async-start(), calls=%async_computation.13 | async-start | bytes 589824 | tf_op jit(solution)/shard_map/reduce_scatter | solution.py:156
  209.8 55.5 %copy-start.13 = (f32[320,256]{1,0:T(8,128)}, f32[320,256]{1,0:T(8,128)S(1)}, u32[]{:S(2)}) copy-start(f32[320,256]{1,0:T(8,128)S(1)} %fusion.29) | copy-start | bytes 983044
  265.3 1.6 copy-start.11
  265.3 1.6 copy-start.14
  266.9 1.7 copy-start.5
  266.9 2.0 copy-start.12
  267.4 2.8 copy-start.4
  271.1 50.5 %copy-start.15 = (f32[320,256]{1,0:T(8,128)S(1)}, f32[320,256]{1,0:T(8,128)}, u32[]{:S(2)}) copy-start(f32[320,256]{1,0:T(8,128)} %copy-done.13) | copy-start | bytes 983044
  277.3 8.5 %all-to-all-start.4 = ((bf16[8,1,160]{2,1,0:T(2,128)(2,1)}), bf16[8,1,160]{2,1,0:T(2,128)(2,1)S(1)}, u32[]{:S(2)}, u32[]{:S(2)}) async-start(bf16[8,1,160]{2,1,0:T(2,128)(2,1)} %all_to_all.25), calls=%async_computation.5 | async-start | bytes 16384 | tf_op jit(solution)/shard_map/all_to_all | solution.py:107
  282.6 79.8 %copy-start.19 = (bf16[1280,512]{0,1:T(8,128)(2,1)S(1)}, bf16[1280,512]{0,1:T(8,128)(2,1)}, u32[]{:S(2)}) copy-start(bf16[1280,512]{0,1:T(8,128)(2,1)} %copy-done.18) | copy-start | bytes 3932164
  316.1 70.7 %all-to-all-start.3 = ((bf16[8,160,512]{2,1,0:T(8,128)(2,1)}), bf16[8,160,512]{2,1,0:T(8,128)(2,1)S(1)}, u32[]{:S(2)}, u32[]{:S(2)}) async-start(bf16[8,160,512]{2,1,0:T(8,128)(2,1)} %reduce-scatter.4.cloned.1.call-done), calls=%async_computation.4 | async-start | bytes 2621440 | tf_op jit(solution)/shard_map/all_to_all | solution.py:106
  321.6 131.1 %reduce-scatter.8.cloned.1.call-start = ((), (), s32[]{:S(2)}) async-start(), calls=%async_computation.14 | async-start | bytes 589824 | tf_op jit(solution)/shard_map/reduce_scatter | solution.py:157
  362.4 7.3 %copy-start.17 = (bf16[1280,512]{0,1:T(8,128)(2,1)S(1)}, bf16[1280,512]{0,1:T(8,128)(2,1)}, u32[]{:S(2)}) copy-start(bf16[1280,512]{0,1:T(8,128)(2,1)} %copy-done.16) | copy-start | bytes 3932164
  362.4 14.5 %slice-start = ((s8[5242880]{0:T(1024)(128)(4,1)}), s8[4194304]{0:T(1024)(128)(4,1)S(1)}, s32[]{:S(2)}) async-start(s8[5242880]{0:T(1024)(128)(4,1)} %bitcast.78), calls=%async_computation.15 | async-start | bytes 8388608
  369.6 7.2 %slice-start.1 = ((s8[5242880]{0:T(1024)(128)(4,1)}), s8[1048576]{0:T(1024)(128)(4,1)S(1)}, s32[]{:S(2)}) async-start(s8[5242880]{0:T(1024)(128)(4,1)} %bitcast.78), calls=%async_computation.16 | async-start | bytes 2097152
  369.6 7.2 %copy-start.20 = (bf16[1280,512]{0,1:T(8,128)(2,1)S(1)}, bf16[1280,512]{0,1:T(8,128)(2,1)}, u32[]{:S(2)}) copy-start(bf16[1280,512]{0,1:T(8,128)(2,1)} %get-tuple-element.37) | copy-start | bytes 3932164
  386.8 65.9 %copy-start.1 = (bf16[1,2048,512]{2,1,0:T(8,128)(2,1)S(1)}, bf16[1,2048,512]{2,1,0:T(8,128)(2,1)}, u32[]{:S(2)}) copy-start(bf16[1,2048,512]{2,1,0:T(8,128)(2,1)} %param.14) | copy-start | bytes 6291460
Sparse Core Ops, SparseCore 0:
  67.3 42.9 all-gather.8
  111.9 40.3 all-gather.10
  155.2 52.8 all-gather.6
  210.8 52.5 all-gather.4
  265.8 50.3 reduce-scatter.3
  319.9 67.5 reduce-scatter.5
  391.4 61.2 reduce-scatter.7
where the time goes:
time: 464 us; the launch traced here: 460 us
  waiting for transfers between devices  200 us (43%)
  blocking collectives  113 us (24%)
  matrix products  58.6 us (13%)
  local copies, waits for them, and re-layouts  45.7 us (10%)
  starting transfers between devices  17.5 us (4%)
  between operations  15.2 us (3%)
  other arithmetic  10.1 us (2%)
    reduce_scatter x1, waiting for transfers between devices, shards(): lax.psum_scatter(out_partial, 'ep', scatter_dimension=0, tiled=True)  55.9 us
    all_gather x1, waiting for transfers between devices, shards(): lax.all_gather(dense_out, ('ep', 'tp'), axis=0, tiled=True)  53.6 us
    unnamed x1, blocking collectives  38.9 us
    all_to_all x1, blocking collectives, shards(): lax.all_to_all(dy_part, 'ep', split_axis=0, concat_axis=0, tiled=True)  34.5 us
    all_gather x1, waiting for transfers between devices, shards(): lax.all_gather(dense_in, ('ep', 'tp'), axis=0, tiled=True)  33.9 us
    all_to_all x1, blocking collectives, shards(): lax.all_to_all(x_part, 'ep', split_axis=0, concat_axis=0, tiled=True)  33.9 us
    reduce_scatter x1, waiting for transfers between devices, shards(): lax.psum_scatter(row_partial.reshape(count_ep, capacity, model_width).ast...  30.3 us
    all_gather x1, waiting for transfers between devices, shards(): lax.all_gather(dy_quarter, 'tp', axis=2, tiled=True)  18.9 us
  transfers between devices with their start and end apart: 10, of which 7 were waited for; matrix products, arithmetic and copies ran while one was open for 19% of the time, Pallas kernels for 0%

commit v1 on v0

v1 whole, which is shorter than its diff:
```python
import functools

import jax
import jax.numpy as jnp
from jax import lax
from jax.experimental import pallas as pl
from jax.experimental.pallas import tpu as pltpu
from jax.sharding import PartitionSpec as P

CLAMP_LIMIT = 7.0
SIG_SLOPE = 1.702
MESH = pl.DeviceIdType.MESH
ANY = pl.BlockSpec(memory_space=pl.ANY)
VMEM = pl.BlockSpec(memory_space=pltpu.VMEM)


def greet(devices):
    barrier = pltpu.get_barrier_semaphore()
    for device in devices:
        pl.semaphore_signal(barrier, inc=1, device_id=device, device_id_type=MESH)
    pl.semaphore_wait(barrier, len(devices))


def dispatch_kernel(
    n_ep,
    x_quarter,
    dy_quarter,
    x_own,
    dy_own,
    weight_rows,
    in_own,
    out_own,
    x_all,
    dy_all,
    weight_all,
    in_all,
    out_all,
    own_buf,
    shard_buf,
    local_sem,
    send_rows,
    recv_rows,
    send_shard,
    recv_shard,
    send_w,
    recv_w,
):
    me = lax.axis_index("ep")
    t = lax.axis_index("tp")
    half = t // 2
    side = t % 2
    t_core = half * 2 + 1 - side
    t_x = (1 - half) * 2 + side
    cols = x_quarter.shape[2]

    def ahead(k):
        return lax.rem(me + k, n_ep)

    def behind(k):
        return lax.rem(me + n_ep - k, n_ep)

    core_peer = (me, t_core)
    x_peer = (me, t_x)
    greet([(ahead(k), t) for k in range(1, n_ep)] + [core_peer, x_peer])

    rows_in = (x_quarter, dy_quarter)
    rows_out = (x_all, dy_all)
    shards_in = (in_own, out_own)
    shards_out = (in_all, out_all)

    def row_slice(a, i, q):
        return rows_out[a].at[i, :, pl.ds(pl.multiple_of(q * cols, cols), cols)]

    def copy_to(src, dst, send, recv, device):
        return pltpu.make_async_remote_copy(
            src_ref=src,
            dst_ref=dst,
            send_sem=send,
            recv_sem=recv,
            device_id=device,
            device_id_type=MESH,
        )

    started = []

    def go(copy):
        copy.start()
        started.append(copy)
        return copy

    def shard_hop(a, kind, k, src_i, first=False):
        if kind == 0:
            return copy_to(
                shards_in[a],
                shards_out[a].at[me, t],
                send_shard.at[a, 0, k],
                recv_shard.at[a, 0, k],
                (ahead(k), t),
            )
        own = shards_in[a] if first else shards_out[a].at[src_i, t]
        if kind == 1:
            return copy_to(
                own,
                shards_out[a].at[src_i, t],
                send_shard.at[a, 1, k],
                recv_shard.at[a, 1, k],
                x_peer,
            )
        if kind == 2:
            return copy_to(
                own,
                shards_out[a].at[src_i, t],
                send_shard.at[a, 2, k],
                recv_shard.at[a, 2, k],
                core_peer,
            )
        return copy_to(
            shards_out[a].at[src_i, t_x],
            shards_out[a].at[src_i, t_x],
            send_shard.at[a, 3, k],
            recv_shard.at[a, 3, k],
            core_peer,
        )

    def row_hop(a, kind, k, i):
        if kind == 0:
            return copy_to(
                rows_in[a].at[ahead(k)],
                row_slice(a, me, t),
                send_rows.at[a, 0, k],
                recv_rows.at[a, 0, k],
                (ahead(k), t),
            )
        if kind == 3:
            return copy_to(
                row_slice(a, i, t_x),
                row_slice(a, i, t_x),
                send_rows.at[a, 3, k],
                recv_rows.at[a, 3, k],
                core_peer,
            )
        return copy_to(
            row_slice(a, i, t),
            row_slice(a, i, t),
            send_rows.at[a, kind, k],
            recv_rows.at[a, kind, k],
            x_peer if kind == 1 else core_peer,
        )

    def w_hop(k):
        return copy_to(
            weight_rows.at[ahead(k)],
            weight_all.at[me],
            send_w.at[k],
            recv_w.at[k],
            (ahead(k), t),
        )

    for a in range(2):
        go(shard_hop(a, 1, 0, me, True))
        go(shard_hop(a, 2, 0, me, True))
    for k in range(1, n_ep):
        for a in range(2):
            go(shard_hop(a, 0, k, me))
        go(w_hop(k))
        for a in range(2):
            go(row_hop(a, 0, k, me))

    ins = [
        pltpu.make_async_copy(x_own, own_buf.at[0], local_sem.at[0]),
        pltpu.make_async_copy(dy_own, own_buf.at[1], local_sem.at[1]),
        pltpu.make_async_copy(in_own, shard_buf.at[0], local_sem.at[2]),
        pltpu.make_async_copy(out_own, shard_buf.at[1], local_sem.at[3]),
    ]
    outs = [
        pltpu.make_async_copy(own_buf.at[0], x_all.at[me], local_sem.at[4]),
        pltpu.make_async_copy(own_buf.at[1], dy_all.at[me], local_sem.at[5]),
        pltpu.make_async_copy(shard_buf.at[0], in_all.at[me, t], local_sem.at[6]),
        pltpu.make_async_copy(shard_buf.at[1], out_all.at[me, t], local_sem.at[7]),
    ]
    for c in ins:
        c.start()
    weight_all[pl.ds(me, 1)] = weight_rows[pl.ds(me, 1)]
    for c, o in zip(ins, outs):
        c.wait()
        o.start()

    def relay(k):
        i = behind(k)
        for a in range(2):
            shard_hop(a, 1, k, i).wait_recv()
            go(shard_hop(a, 3, k, i))
            if k > 0:
                row_hop(a, 1, k, i).wait_recv()
                go(row_hop(a, 3, k, i))

    for k in range(1, n_ep):
        i = behind(k)
        for a in range(2):
            shard_hop(a, 0, k, i).wait_recv()
            go(shard_hop(a, 1, k, i))
            go(shard_hop(a, 2, k, i))
            row_hop(a, 0, k, i).wait_recv()
            go(row_hop(a, 1, k, i))
            go(row_hop(a, 2, k, i))
        relay(k - 1)
    relay(n_ep - 1)

    for k in range(n_ep):
        i = behind(k)
        for a in range(2):
            for kind in (2, 3):
                shard_hop(a, kind, k, i).wait_recv()
                if k > 0:
                    row_hop(a, kind, k, i).wait_recv()
        if k > 0:
            w_hop(k).wait_recv()
    for c in started:
        c.wait_send()
    for o in outs:
        o.wait()


def return_kernel(
    n_ep,
    n_tp,
    part,
    grad_in,
    grad_out,
    grad_gate,
    weight_part,
    rows_back,
    in_back,
    out_back,
    gate_back,
    weight_back,
    from_core,
    to_x,
    from_x,
    to_ep,
    send_core,
    recv_core,
    send_x,
    recv_x,
    send_ep,
    recv_ep,
    send_grad,
    recv_grad,
    send_w,
    recv_w,
):
    me = lax.axis_index("ep")
    t = lax.axis_index("tp")
    half = t // 2
    side = t % 2
    t_core = half * 2 + 1 - side
    t_x = (1 - half) * 2 + side
    cols = rows_back.shape[2]

    def ahead(k):
        return lax.rem(me + k, n_ep)

    def quarter(q):
        return pl.ds(pl.multiple_of(q * cols, cols), cols)

    core_peer = (me, t_core)
    x_peer = (me, t_x)
    others = [
        (ahead(k), lax.rem(t + d, n_tp))
        for k in range(n_ep)
        for d in range(n_tp)
        if k > 0 or d > 0
    ]
    greet(others)

    def copy_to(src, dst, send, recv, device):
        return pltpu.make_async_remote_copy(
            src_ref=src,
            dst_ref=dst,
            send_sem=send,
            recv_sem=recv,
            device_id=device,
            device_id_type=MESH,
        )

    started = []

    def go(copy):
        copy.start()
        started.append(copy)

    order = list(range(1, n_ep)) + [0]

    def core_hop(k, h):
        j = ahead(k)
        return copy_to(
            part.at[j, :, quarter(h * 2 + 1 - side)],
            from_core.at[k, h],
            send_core.at[k, h],
            recv_core.at[k, h],
            core_peer,
        )

    def x_hop(k):
        return copy_to(to_x.at[k], from_x.at[k], send_x.at[k], recv_x.at[k], x_peer)

    def ep_hop(k):
        return copy_to(
            to_ep.at[k], rows_back.at[me], send_ep.at[k], recv_ep.at[k], (ahead(k), t)
        )

    for k in order:
        for h in range(2):
            go(core_hop(k, h))
    grads = ((grad_in, in_back), (grad_out, out_back), (grad_gate, gate_back))

    def grad_hop(a, k):
        src, dst = grads[a]
        return copy_to(
            src.at[ahead(k)],
            dst.at[me],
            send_grad.at[a, k],
            recv_grad.at[a, k],
            (ahead(k), t),
        )

    def w_hop(k, d):
        return copy_to(
            weight_part.at[ahead(k)],
            weight_back.at[me, t],
            send_w.at[k, d],
            recv_w.at[k, d],
            (ahead(k), lax.rem(t + d, n_tp)),
        )

    for k in range(n_ep):
        for d in range(n_tp):
            if k > 0 or d > 0:
                go(w_hop(k, d))
        if k > 0:
            for a in range(3):
                go(grad_hop(a, k))
    for a in range(3):
        grads[a][1][pl.ds(me, 1)] = grads[a][0][pl.ds(me, 1)]
    weight_back[pl.ds(me, 1), pl.ds(t, 1)] = weight_part[pl.ds(me, 1)][:, None]

    def finish(k):
        j = ahead(k)
        x_hop(k).wait_recv()
        mine = part[j, :, quarter(t)].astype(jnp.float32)
        mine = mine + from_core[k, half].astype(jnp.float32)
        mine = (mine + from_x[k].astype(jnp.float32)).astype(jnp.bfloat16)
        if k > 0:
            to_ep[k] = mine
            go(ep_hop(k))
        else:
            rows_back[me] = mine

    lag = 2
    for n, k in enumerate(order):
        j = ahead(k)
        for h in range(2):
            core_hop(k, h).wait_recv()
        other = part[j, :, quarter(t_x)].astype(jnp.float32)
        other = other + from_core[k, 1 - half].astype(jnp.float32)
        to_x[k] = other.astype(jnp.bfloat16)
        go(x_hop(k))
        if n >= lag:
            finish(order[n - lag])
    for k in order[n_ep - lag :]:
        finish(k)

    for k in range(n_ep):
        if k > 0:
            ep_hop(k).wait_recv()
            for a in range(3):
                grad_hop(a, k).wait_recv()
        for d in range(n_tp):
            if k > 0 or d > 0:
                w_hop(k, d).wait_recv()
    for c in started:
        c.wait_send()


def dispatch(n_ep, n_tp, *args):
    x_quarter, dy_quarter, x_own, dy_own, weight_rows, in_own, out_own = args
    cap, cols = x_quarter.shape[1:]
    width = x_own.shape[1]
    bf = jnp.bfloat16
    dma = pltpu.SemaphoreType.DMA
    rows = jax.ShapeDtypeStruct((n_ep, cap, width), bf)
    shard = jax.ShapeDtypeStruct((n_ep, n_tp) + in_own.shape, bf)
    return pl.pallas_call(
        functools.partial(dispatch_kernel, n_ep),
        out_shape=(
            rows,
            rows,
            jax.ShapeDtypeStruct(weight_rows.shape, weight_rows.dtype),
            shard,
            shard,
        ),
        in_specs=[ANY, ANY, ANY, ANY, VMEM, ANY, ANY],
        out_specs=(ANY, ANY, VMEM, ANY, ANY),
        scratch_shapes=[
            pltpu.VMEM((2, cap, width), bf),
            pltpu.VMEM((2,) + in_own.shape, bf),
            dma((8,)),
            dma((2, 4, n_ep)),
            dma((2, 4, n_ep)),
            dma((2, 4, n_ep)),
            dma((2, 4, n_ep)),
            dma((n_ep,)),
            dma((n_ep,)),
        ],
        compiler_params=pltpu.CompilerParams(collective_id=0, has_side_effects=True),
        name="dispatch",
    )(*args)


def give_back(n_ep, n_tp, *args):
    part, grad_in, grad_out, grad_gate, weight_part = args
    cap, width = part.shape[1:]
    cols = width // n_tp
    bf = jnp.bfloat16
    dma = pltpu.SemaphoreType.DMA
    same = lambda a: jax.ShapeDtypeStruct(a.shape, a.dtype)
    return pl.pallas_call(
        functools.partial(return_kernel, n_ep, n_tp),
        out_shape=(
            jax.ShapeDtypeStruct((n_ep, cap, cols), bf),
            same(grad_in),
            same(grad_out),
            same(grad_gate),
            jax.ShapeDtypeStruct((n_ep, n_tp) + weight_part.shape[1:], weight_part.dtype),
        ),
        in_specs=[VMEM] * 5,
        out_specs=(VMEM,) * 5,
        scratch_shapes=[
            pltpu.VMEM((n_ep, 2, cap, cols), bf),
            pltpu.VMEM((n_ep, cap, cols), bf),
            pltpu.VMEM((n_ep, cap, cols), bf),
            pltpu.VMEM((n_ep, cap, cols), bf),
            dma((n_ep, 2)),
            dma((n_ep, 2)),
            dma((n_ep,)),
            dma((n_ep,)),
            dma((n_ep,)),
            dma((n_ep,)),
            dma((3, n_ep)),
            dma((3, n_ep)),
            dma((n_ep, n_tp)),
            dma((n_ep, n_tp)),
        ],
        compiler_params=pltpu.CompilerParams(
            collective_id=1, has_side_effects=True, vmem_limit_bytes=40 * 1024 * 1024
        ),
        name="give_back",
    )(*args)


def shards(
    tokens,
    cotangent,
    route_ids,
    route_weights,
    w_gate,
    w_up,
    w_down,
    dense_in,
    dense_out,
    dense_gate,
):
    count_ep = lax.axis_size("ep")
    count_tp = lax.axis_size("tp")
    ep_index = lax.axis_index("ep")
    tp_index = lax.axis_index("tp")
    tok_dev, model_width = tokens.shape
    top_k = route_ids.shape[1]
    col_count = model_width // count_tp
    capacity = 2 * tok_dev * top_k // count_ep
    lanes = -(-capacity // 128) * 128
    slot_total = count_ep * capacity
    bf = jnp.bfloat16
    f32 = jnp.float32

    names = jnp.arange(count_ep, dtype=jnp.int32)
    chosen = route_ids[:, :, None] == names[None, None, :]
    member = jnp.any(chosen, axis=1).astype(bf)
    row = jnp.arange(tok_dev, dtype=jnp.int32)
    below = (row[None, :] < row[:, None]).astype(bf)
    rank = jnp.dot(below, member, preferred_element_type=f32)
    slot_index = jnp.sum(jnp.where(chosen, rank[:, None, :], 0.0), axis=2).astype(jnp.int32)
    target = route_ids * capacity + slot_index
    lane_target = route_ids * lanes + slot_index
    slots = jnp.arange(slot_total, dtype=jnp.int32)
    pick = slots[:, None] == target[:, 0][None, :]
    for k in range(1, top_k):
        pick = pick | (slots[:, None] == target[:, k][None, :])
    pick = pick.astype(bf)
    tok_part = lax.dynamic_slice_in_dim(tokens, tp_index * col_count, col_count, 1)
    cot_part = lax.dynamic_slice_in_dim(cotangent, tp_index * col_count, col_count, 1)
    quarter_shape = (count_ep, capacity, col_count)
    x_quarter = jnp.dot(pick, tok_part, preferred_element_type=bf).reshape(quarter_shape)
    dy_quarter = jnp.dot(pick, cot_part, preferred_element_type=bf).reshape(quarter_shape)
    pick_own = lax.dynamic_slice_in_dim(pick, ep_index * capacity, capacity, 0)
    x_own = jnp.dot(pick_own, tokens, preferred_element_type=bf)
    dy_own = jnp.dot(pick_own, cotangent, preferred_element_type=bf)
    lane_slots = jnp.arange(count_ep * lanes, dtype=jnp.int32)
    lane_hits = lane_target[:, :, None] == lane_slots[None, None, :]
    weight_rows = jnp.sum(
        jnp.where(lane_hits, route_weights.astype(f32)[:, :, None], 0.0), axis=(0, 1)
    ).astype(bf)
    weight_rows = jnp.broadcast_to(
        weight_rows.reshape(count_ep, 1, lanes), (count_ep, 16, lanes)
    )
    x_in, dy_in, weight_in, in_all, out_all = dispatch(
        count_ep, count_tp, x_quarter, dy_quarter, x_own, dy_own, weight_rows, dense_in, dense_out
    )
    in_whole = in_all.reshape(model_width, -1)
    out_whole = out_all.reshape(model_width, -1)

    x_slots = x_in.reshape(slot_total, model_width)
    dy_slots = dy_in.reshape(slot_total, model_width)
    route_col = weight_in[:, 0, :capacity].reshape(slot_total, 1).astype(f32)
    gate_w = w_gate[0]
    up_w = w_up[0]
    down_w = w_down[0]
    gate_pre = jnp.dot(x_slots, gate_w, preferred_element_type=f32)
    up_pre = jnp.dot(x_slots, up_w, preferred_element_type=f32)
    gate_clamp = jnp.minimum(gate_pre, CLAMP_LIMIT)
    up_clamp = jnp.clip(up_pre, -CLAMP_LIMIT, CLAMP_LIMIT)
    sig = jax.nn.sigmoid(SIG_SLOPE * gate_clamp)
    act = (gate_clamp * sig * (up_clamp + 1.0)).astype(bf)
    back = lax.dot_general(
        dy_slots, down_w, (((1,), (1,)), ((), ())), preferred_element_type=f32
    )
    d_act = route_col * back
    d_gate = jnp.where(
        gate_pre < CLAMP_LIMIT,
        d_act * (up_clamp + 1.0) * (sig + SIG_SLOPE * gate_clamp * sig * (1.0 - sig)),
        0.0,
    ).astype(bf)
    d_up = jnp.where(jnp.abs(up_pre) < CLAMP_LIMIT, d_act * gate_clamp * sig, 0.0).astype(bf)
    scaled_cot = (route_col * dy_slots.astype(f32)).astype(bf)
    contract_rows = (((0,), (0,)), ((), ()))
    grad_gate = lax.dot_general(x_slots, d_gate, contract_rows, preferred_element_type=f32)
    grad_up = lax.dot_general(x_slots, d_up, contract_rows, preferred_element_type=f32)
    grad_down = lax.dot_general(act, scaled_cot, contract_rows, preferred_element_type=f32)
    contract_cols = (((1,), (1,)), ((), ()))
    row_partial = lax.dot_general(d_gate, gate_w, contract_cols, preferred_element_type=f32)
    row_partial = row_partial + lax.dot_general(
        d_up, up_w, contract_cols, preferred_element_type=f32
    )
    part = row_partial.astype(bf).reshape(count_ep, capacity, model_width)
    weight_part = jnp.sum(act.astype(f32) * back, axis=1).reshape(count_ep, capacity)
    weight_part = jnp.pad(weight_part, ((0, 0), (0, lanes - capacity)))
    weight_part = jnp.broadcast_to(weight_part[:, None, :], (count_ep, 8, lanes))

    dense_pre = jnp.dot(tokens, in_whole, preferred_element_type=f32)
    dense_act = jax.nn.silu(dense_pre).astype(bf)
    dense_val = lax.dot_general(dense_act, out_whole, contract_cols, preferred_element_type=f32)
    mix = jax.nn.sigmoid(jnp.dot(tokens, dense_gate, preferred_element_type=f32))
    cot_wide = cotangent.astype(f32)
    dense_scaled = (mix[:, None] * cot_wide).astype(bf)
    dense_back = jnp.dot(dense_scaled, out_whole, preferred_element_type=f32)
    sig_pre = jax.nn.sigmoid(dense_pre)
    dense_dpre = (dense_back * sig_pre * (1.0 + dense_pre * (1.0 - sig_pre))).astype(bf)
    dlogit = mix * (1.0 - mix) * jnp.sum(cot_wide * dense_val, axis=1)
    in_rows = lax.dynamic_slice_in_dim(in_whole, tp_index * col_count, col_count, 0)
    gate_cols = lax.dynamic_slice_in_dim(dense_gate, tp_index * col_count, col_count, 0)
    dense_dx = lax.dot_general(dense_dpre, in_rows, contract_cols, preferred_element_type=f32)
    dense_dx = dense_dx + dlogit[:, None] * gate_cols.astype(f32)[None, :]
    block_cols = model_width // (count_ep * count_tp)
    tokens_own = lax.dynamic_index_in_dim(
        tokens.reshape(tok_dev, count_ep, count_tp, block_cols), tp_index, 2, keepdims=False
    ).reshape(tok_dev, count_ep * block_cols)
    scaled_own = lax.dynamic_index_in_dim(
        dense_scaled.reshape(tok_dev, count_ep, count_tp, block_cols), tp_index, 2, keepdims=False
    ).reshape(tok_dev, count_ep * block_cols)
    in_partial = lax.dot_general(tokens_own, dense_dpre, contract_rows, preferred_element_type=f32)
    out_partial = lax.dot_general(scaled_own, dense_act, contract_rows, preferred_element_type=f32)
    gate_partial = jnp.sum(tokens_own.astype(f32) * dlogit[:, None], axis=0)
    gate_partial = jnp.pad(
        gate_partial.reshape(count_ep, 1, block_cols), ((0, 0), (0, 7), (0, -block_cols % 128))
    )

    rows_back, in_back, out_back, gate_back, weight_back = give_back(
        count_ep,
        count_tp,
        part,
        in_partial.reshape(count_ep, block_cols, -1),
        out_partial.reshape(count_ep, block_cols, -1),
        gate_partial,
        weight_part,
    )
    grad_dense_in = jnp.sum(in_back, axis=0)
    grad_dense_out = jnp.sum(out_back, axis=0)
    grad_dense_gate = jnp.sum(gate_back[:, 0, :block_cols], axis=0)
    expert_dx = lax.dot_general(
        pick, rows_back.reshape(slot_total, col_count), contract_rows, preferred_element_type=f32
    )
    grad_tokens = (dense_dx + expert_dx).astype(bf)
    weight_grad = jnp.sum(weight_back[:, :, 0, :], axis=1).reshape(-1)
    grad_route_weights = jnp.sum(
        jnp.where(lane_hits, weight_grad[None, None, :], 0.0), axis=2
    ).astype(bf)
    return (
        grad_tokens,
        grad_route_weights,
        grad_gate[None],
        grad_up[None],
        grad_down[None],
        grad_dense_in,
        grad_dense_out,
        grad_dense_gate,
    )


def solution(mesh):
    placed = (
        P("ep", None),
        P("ep", None),
        P("ep", None),
        P("ep", None),
        P("ep", None, "tp"),
        P("ep", None, "tp"),
        P("ep", "tp", None),
        P(("ep", "tp"), None),
        P(("ep", "tp"), None),
        P(),
    )
    return jax.shard_map(
        shards,
        mesh=mesh,
        in_specs=placed,
        out_specs=(
            P("ep", "tp"),
            P("ep", None),
            P("ep", None, "tp"),
            P("ep", None, "tp"),
            P("ep", "tp", None),
            P(("ep", "tp"), None),
            P(("ep", "tp"), None),
            P(("ep", "tp")),
        ),
        check_vma=False,
    )
```

time: 464 us -> 267 us (0.58)
  waiting for transfers between devices: 200 us -> 0 us
  Pallas kernels: 0 us -> 175 us
  blocking collectives: 113 us -> 0 us
  local copies, waits for them, and re-layouts: 45.7 us -> 8.62 us
  starting transfers between devices: 17.5 us -> 0 us
  between operations: 15.2 us -> 0.88 us
  matrix products: 58.6 us -> 71.3 us
    pallas_call x0 -> x2, Pallas kernels: none -> 175 us  [the longest x1 93.9 us: dispatch(): pl.pallas_call(functools.partial(dispatch_kernel, n_ep), out_shape=(rows,...]
    all_gather x4 -> x0, waiting for transfers between devices: 106 us -> none  [the longest x1 53.6 us: shards(): lax.all_gather(dense_out, ('ep', 'tp'), axis=0, tiled=True)]
    reduce_scatter x3 -> x0, waiting for transfers between devices: 86.1 us -> none  [the longest x1 55.9 us: shards(): lax.psum_scatter(out_partial, 'ep', scatter_dimension=0, tiled=True)]
    all_to_all x2 -> x0, blocking collectives: 68.4 us -> none  [the longest x1 34.5 us: shards(): lax.all_to_all(dy_part, 'ep', split_axis=0, concat_axis=0, tiled=True)]
    unnamed x1 -> x0, blocking collectives: 38.9 us -> none
    gather x5 -> x0, local copies, waits for them, and re-layouts: 34.1 us -> none  [the longest x1 12.4 us: shards(): tokens[token_of]]
    all_to_all x3 -> x0, starting transfers between devices: 17.1 us -> none  [the longest x1 6.45 us: shards(): lax.all_to_all(weight_rows, 'ep', split_axis=0, concat_axis=0, tiled=True)]
    dot_general x10 -> x16, matrix products: 41.7 us -> 57.1 us  [the longest x1 8.15 us: shards(): lax.dot_general(act, scaled_cot, contract_rows, preferred_element_type=f32)]
  transfers between devices with their start and end apart: 10 -> 0, of which waited for: 7 -> 0; matrix products, arithmetic and copies ran while one was open for 19% -> 0% of each run, Pallas kernels for 0% -> 0%
where the time goes in v1:
time: 267 us; the launch traced here: 266 us
  Pallas kernels  175 us (66%)
  matrix products  71.3 us (27%)
  other arithmetic  10.9 us (4%)
  local copies, waits for them, and re-layouts  8.62 us (3%)
    pallas_call x1, Pallas kernels, dispatch(): pl.pallas_call(functools.partial(dispatch_kernel, n_ep), out_shape=(rows,...  93.9 us
    pallas_call x1, Pallas kernels, give_back(): pl.pallas_call(functools.partial(return_kernel, n_ep, n_tp), out_shape=(j...  80.6 us
    dot_general x1, matrix products, shards(): lax.dot_general(dy_slots, down_w, (((1,), (1,)), ((), ())), preferred_ele...  9.69 us
    dot_general x1, matrix products, shards(): lax.dot_general(act, scaled_cot, contract_rows, preferred_element_type=f32)  8.15 us
    dot_general x1, matrix products, shards(): lax.dot_general(x_slots, d_up, contract_rows, preferred_element_type=f32)  7.94 us
    dot_general x1, matrix products, shards(): lax.dot_general(x_slots, d_gate, contract_rows, preferred_element_type=f32)  7.18 us
    dot_general x1, matrix products, shards(): gate_pre = jnp.dot(x_slots, gate_w, preferred_element_type=f32)  7.06 us

profile of v1, /device:TPU:13, one launch (start us, length us, event | category | flops | bytes accessed | tf_op | source)
XLA Modules:
  0.0 266.3 jit_solution(9046552831978979948)
XLA Ops:
  0.6 0.0 copy-start
  0.7 0.9 fusion.36
  1.5 0.1 fusion.18
  1.6 0.8 select_reduce_fusion.2
  2.4 0.7 multiply_add_fusion
  3.1 2.9 %fusion.25 = bf16[1280,512]{1,0:T(8,128)(2,1)} fusion(bf16[320,2048]{1,0:T(8,128)(2,1)} %param.11, s32[]{:T(128)S(6)} %select_n.34, s32[320]{0:T(512)S(1)} %get-tuple-element.29, s32[320]{0:T(512)S(1)} %get-tuple-element.28), kind=kOutput, calls=%fused_computation.52 | convolution fusion | flops 420659200 | bytes 1640964 | tf_op jit(solution)/shard_map/dot_general | solution.py:504
  6.0 1.9 fusion.27
  7.9 1.2 fusion.13
  9.1 2.7 %fusion.30.dy_own = bf16[160,2048]{1,0:T(8,128)(2,1)} fusion(bf16[320,2048]{1,0:T(8,128)(2,1)} %param.11, pred[1280,320]{1,0:T(32,128)(4,1)} %fusion.13, s32[]{:T(128)S(6)} %select_n.35), kind=kOutput, calls=%fused_computation.57 | convolution fusion | flops 209715200 | bytes 2027524 | tf_op jit(solution)/shard_map/dot_general | solution.py:507
  11.9 2.2 fusion.32.x_own
  14.0 0.7 select_reduce_fusion.1
  14.8 0.6 broadcast_in_dim.79.weight_rows
  15.4 93.9 %dispatch.1 = (bf16[8,160,2048]{2,1,0:T(8,128)(2,1)}, bf16[8,160,2048]{2,1,0:T(8,128)(2,1)}, bf16[8,16,256]{2,1,0:T(8,128)(2,1)}, bf16[8,4,64,256]{3,2,1,0:T(8,128)(2,1)}, bf16[8,4,64,256]{3,2,1,0:T(8,128)(2,1)}) custom-call(bf16[8,160,512]{2,1,0:T(8,128)(2,1)} %bitcast.84, bf16[8,160,512]{2,1,0:T(8,128)(2,1)} %bitcast.83, bf16[160,2048]{1,0:T(8,128)(2,1)} %fusion.32.x_own, ...), custom_call_target="tpu_custom_call" | custom-call | tf_op jit(solution)/shard_map/dispatch/pallas_call | solution.py:393
  109.4 0.0 copy-start.11
  109.4 7.1 %fusion.11 = f32[1280,512]{0,1:T(8,128)} fusion(bf16[1280,2048]{1,0:T(8,128)(2,1)} %bitcast.90, bf16[1,2048,512]{2,1,0:T(8,128)(2,1)S(1)} %copy-done), kind=kOutput, calls=%fused_computation.27 | convolution fusion | flops 2684354560 | bytes 9961472 | tf_op jit(solution)/shard_map/dot_general | solution.py:528
  116.5 4.6 %fusion.5 = f32[1280,512]{0,1:T(8,128)} fusion(bf16[1280,2048]{1,0:T(8,128)(2,1)S(1)} %bitcast.93, bf16[1,2048,512]{2,1,0:T(8,128)(2,1)S(1)} %copy-done.11), kind=kOutput, calls=%fused_computation.21 | convolution fusion | flops 2684354560 | bytes 9961472 | tf_op jit(solution)/shard_map/dot_general | solution.py:529
  121.1 0.8 convert_reduce_fusion
  121.9 0.1 reshape.113
  122.0 9.7 %multiply_reduce_fusion = (f32[1280]{0:T(1024)S(1)}, bf16[1280,512]{0,1:T(8,128)(2,1)S(1)}, bf16[1280,512]{0,1:T(8,128)(2,1)S(1)}, bf16[1280,512]{0,1:T(8,128)(2,1)S(1)}) fusion(f32[1280,512]{0,1:T(8,128)} %fusion.5, f32[1280,512]{0,1:T(8,128)} %fusion.11, f32[1280]{0:T(1024)S(1)} %reshape.113, bf16[1280,2048]{1,0:T(8,128)(2,1)} %bitcast.94, ...), kind=kOutput, calls=%fused_computation.13 | convolution fusion | flops 2703358720 | bytes 16525312 | tf_op jit(solution)/shard_map/dot_general | solution.py:534
  131.7 8.1 %fusion.2 = f32[1,512,2048]{2,1,0:T(8,128)} fusion(bf16[1280,512]{0,1:T(8,128)(2,1)S(1)} %get-tuple-element.31, bf16[1280,2048]{1,0:T(8,128)(2,1)} %bitcast.95, f32[1280]{0:T(1024)S(1)} %reshape.113), kind=kOutput, calls=%fused_computation.9 | convolution fusion | flops 2692218880 | bytes 10753024 | tf_op jit(solution)/shard_map/dot_general | solution.py:548
  139.9 2.9 %fusion.9 = f32[1280,2048]{1,0:T(8,128)S(1)} fusion(bf16[1280,512]{0,1:T(8,128)(2,1)S(1)} %get-tuple-element.34, bf16[1,2048,512]{2,1,0:T(8,128)(2,1)S(1)} %copy-done), kind=kOutput, calls=%fused_computation.25 | convolution fusion | flops 2684354560 | bytes 13893632 | tf_op jit(solution)/shard_map/dot_general | solution.py:550
  142.8 4.8 %add_convert_fusion = bf16[1280,2048]{1,0:T(8,128)(2,1)} fusion(f32[1280,2048]{1,0:T(8,128)S(1)} %fusion.9, bf16[1280,512]{0,1:T(8,128)(2,1)S(1)} %get-tuple-element.35, bf16[1,2048,512]{2,1,0:T(8,128)(2,1)S(1)} %copy-done.12), kind=kOutput, calls=%fused_computation.1 | convolution fusion | flops 2689597440 | bytes 19136512 | tf_op jit(solution)/shard_map/dot_general | solution.py:551
  147.6 0.5 convolution_bitcast_fusion.2
  148.1 0.8 copy-done.4
  148.9 0.3 copy-done.13
  149.2 0.7 fusion.14
  149.9 0.0 copy-done.8
  149.9 0.5 convolution_reduce_fusion
  150.4 1.3 fusion.3
  151.8 2.5 copy.30
  154.3 1.3 fusion.19.grad_out
  155.6 0.1 reshape.111
  155.7 2.1 fusion.17
  157.9 0.0 copy-start.5
  157.9 1.6 copy.29
  159.4 1.3 fusion.21.grad_in
  160.7 1.2 multiply_reduce_fusion.1
  161.9 2.5 copy-done.2
  164.4 80.6 %give_back.1 = (bf16[8,160,512]{2,1,0:T(8,128)(2,1)S(1)}, f32[8,64,256]{2,1,0:T(8,128)S(1)}, f32[8,64,256]{2,1,0:T(8,128)S(1)}, f32[8,8,128]{2,1,0:T(8,128)S(1)}, f32[8,4,8,256]{3,2,1,0:T(8,128)S(1)}) custom-call(bf16[8,160,2048]{2,1,0:T(8,128)(2,1)S(1)} %bitcast.78, f32[8,64,256]{2,1,0:T(8,128)S(1)} %fusion.21.grad_in, f32[8,64,256]{2,1,0:T(8,128)S(1)} %fusion.19.grad_out, ...), custom_call_target="tpu_custom_call" | custom-call | tf_op jit(solution)/shard_map/give_back/pallas_call | solution.py:427
  245.0 0.1 dynamic-slice_convert_fusion
  245.1 1.2 convolution_add_fusion.1
  246.3 1.5 fusion.15
  247.9 0.7 reduce_sum.97
  248.5 0.7 reduce_sum.98
  249.2 1.4 select_reduce_fusion
  250.6 0.5 slice_reduce_fusion.1
  251.2 7.9 %convolution_bitcast_fusion = f32[1,2048,512]{2,1,0:T(8,128)} fusion(bf16[1280,2048]{1,0:T(8,128)(2,1)} %bitcast.91, bf16[1280,512]{0,1:T(8,128)(2,1)} %copy-done.16), kind=kOutput, calls=%fused_computation.10 | convolution fusion | flops 2684354560 | bytes 10747904 | tf_op jit(solution)/shard_map/dot_general | solution.py:547
  259.1 7.2 %convolution_bitcast_fusion.1 = f32[1,2048,512]{2,1,0:T(8,128)} fusion(bf16[1280,2048]{1,0:T(8,128)(2,1)} %bitcast.92, bf16[1280,512]{0,1:T(8,128)(2,1)S(1)} %copy-done.15), kind=kOutput, calls=%fused_computation.11 | convolution fusion | flops 2684354560 | bytes 10747904 | tf_op jit(solution)/shard_map/dot_general | solution.py:546
  (37 shorter events, 0.2 us)
Async XLA Ops:
  0.6 108.8 %copy-start = (bf16[1,2048,512]{2,1,0:T(8,128)(2,1)S(1)}, bf16[1,2048,512]{2,1,0:T(8,128)(2,1)}, u32[]{:S(2)}) copy-start(bf16[1,2048,512]{2,1,0:T(8,128)(2,1)} %param.14) | copy-start | bytes 6291460
  0.6 5.4 %copy-start.3 = (bf16[320,2048]{1,0:T(8,128)(2,1)S(1)}, bf16[320,2048]{1,0:T(8,128)(2,1)}, u32[]{:S(2)}) copy-start(bf16[320,2048]{1,0:T(8,128)(2,1)} %param.10) | copy-start | bytes 3932164
  9.1 4.9 %copy-start.9 = (bf16[320,2]{0,1:T(2,128)(2,1)S(1)}, bf16[320,2]{0,1:T(2,128)(2,1)}, u32[]{:S(2)}) copy-start(bf16[320,2]{0,1:T(2,128)(2,1)} %param.13) | copy-start | bytes 3844
  109.4 7.1 %copy-start.10 = (bf16[8,160,2048]{2,1,0:T(8,128)(2,1)S(1)}, bf16[8,160,2048]{2,1,0:T(8,128)(2,1)}, u32[]{:S(2)}) copy-start(bf16[8,160,2048]{2,1,0:T(8,128)(2,1)} %get-tuple-element.20) | copy-start | bytes 15728644
  109.4 7.1 %copy-start.11 = (bf16[1,2048,512]{2,1,0:T(8,128)(2,1)S(1)}, bf16[1,2048,512]{2,1,0:T(8,128)(2,1)}, u32[]{:S(2)}) copy-start(bf16[1,2048,512]{2,1,0:T(8,128)(2,1)} %param.15) | copy-start | bytes 6291460
  131.7 8.2 %copy-start.14 = (bf16[1280,512]{0,1:T(8,128)(2,1)}, bf16[1280,512]{0,1:T(8,128)(2,1)S(1)}, u32[]{:S(2)}) copy-start(bf16[1280,512]{0,1:T(8,128)(2,1)S(1)} %get-tuple-element.34) | copy-start | bytes 3932164
  131.7 11.1 %copy-start.16 = (bf16[1280,512]{0,1:T(8,128)(2,1)}, bf16[1280,512]{0,1:T(8,128)(2,1)S(1)}, u32[]{:S(2)}) copy-start(bf16[1280,512]{0,1:T(8,128)(2,1)S(1)} %get-tuple-element.35) | copy-start | bytes 3932164
  139.8 3.0 %copy-start.12 = (bf16[1,2048,512]{2,1,0:T(8,128)(2,1)S(1)}, bf16[1,2048,512]{2,1,0:T(8,128)(2,1)}, u32[]{:S(2)}) copy-start(bf16[1,2048,512]{2,1,0:T(8,128)(2,1)} %param.15) | copy-start | bytes 6291460
  142.8 4.8 %copy-start.7 = (bf16[8,4,64,256]{3,2,1,0:T(8,128)(2,1)S(1)}, bf16[8,4,64,256]{3,2,1,0:T(8,128)(2,1)}, u32[]{:S(2)}) copy-start(bf16[8,4,64,256]{3,2,1,0:T(8,128)(2,1)} %get-tuple-element.19) | copy-start | bytes 3145732
  147.6 1.3 copy-start.4
  147.6 1.6 copy-start.13
  149.2 0.7 copy-start.8
  157.9 4.0 %copy-start.5 = (bf16[320,256]{1,0:T(8,128)(2,1)}, bf16[320,256]{1,0:T(8,128)(2,1)S(1)}, u32[]{:S(2)}) copy-start(bf16[320,256]{1,0:T(8,128)(2,1)S(1)} %fusion.17) | copy-start | bytes 491524
  161.9 2.5 copy-start.2
  164.4 80.7 %copy-start.6 = (bf16[320,256]{1,0:T(8,128)(2,1)S(1)}, bf16[320,256]{1,0:T(8,128)(2,1)}, u32[]{:S(2)}) copy-start(bf16[320,256]{1,0:T(8,128)(2,1)} %copy-done.5) | copy-start | bytes 491524
  251.2 7.9 %copy-start.15 = (bf16[1280,512]{0,1:T(8,128)(2,1)S(1)}, bf16[1280,512]{0,1:T(8,128)(2,1)}, u32[]{:S(2)}) copy-start(bf16[1280,512]{0,1:T(8,128)(2,1)} %copy-done.14) | copy-start | bytes 3932164
  259.1 7.2 %copy-start.1 = (bf16[1,2048,512]{2,1,0:T(8,128)(2,1)S(1)}, bf16[1,2048,512]{2,1,0:T(8,128)(2,1)}, u32[]{:S(2)}) copy-start(bf16[1,2048,512]{2,1,0:T(8,128)(2,1)} %param.14) | copy-start | bytes 6291460

commit v2 on v1

--- a/solution.py
+++ b/solution.py
@@ -30,12 +30,20 @@
     weight_rows,
     in_own,
     out_own,
+    gate_w,
+    up_w,
+    down_w,
     x_all,
+    scaled_all,
+    act_all,
+    dgate_all,
+    dup_all,
+    part_all,
+    weight_part,
+    in_all,
+    out_all,
     dy_all,
     weight_all,
-    in_all,
-    out_all,
-    own_buf,
     shard_buf,
     local_sem,
     send_rows,
@@ -51,7 +59,10 @@
     side = t % 2
     t_core = half * 2 + 1 - side
     t_x = (1 - half) * 2 + side
-    cols = x_quarter.shape[2]
+    cap, cols = x_quarter.shape[1:]
+    lanes = weight_rows.shape[2]
+    f32 = jnp.float32
+    bf = jnp.bfloat16
 
     def ahead(k):
         return lax.rem(me + k, n_ep)
@@ -81,144 +92,156 @@
             device_id_type=MESH,
         )
 
-    started = []
-
-    def go(copy):
-        copy.start()
-        started.append(copy)
-        return copy
-
-    def shard_hop(a, kind, k, src_i, first=False):
+    def shard_hop(a, kind, k, first=False):
+        i = behind(k)
+        sems = (send_shard.at[a, kind, k], recv_shard.at[a, kind, k])
         if kind == 0:
-            return copy_to(
-                shards_in[a],
-                shards_out[a].at[me, t],
-                send_shard.at[a, 0, k],
-                recv_shard.at[a, 0, k],
-                (ahead(k), t),
-            )
-        own = shards_in[a] if first else shards_out[a].at[src_i, t]
-        if kind == 1:
-            return copy_to(
-                own,
-                shards_out[a].at[src_i, t],
-                send_shard.at[a, 1, k],
-                recv_shard.at[a, 1, k],
-                x_peer,
-            )
-        if kind == 2:
-            return copy_to(
-                own,
-                shards_out[a].at[src_i, t],
-                send_shard.at[a, 2, k],
-                recv_shard.at[a, 2, k],
-                core_peer,
-            )
+            return copy_to(shards_in[a], shards_out[a].at[me, t], *sems, (ahead(k), t))
+        if kind == 3:
+            block = shards_out[a].at[i, t_x]
+            return copy_to(block, block, *sems, core_peer)
+        block = shards_out[a].at[i, t]
         return copy_to(
-            shards_out[a].at[src_i, t_x],
-            shards_out[a].at[src_i, t_x],
-            send_shard.at[a, 3, k],
-            recv_shard.at[a, 3, k],
-            core_peer,
-        )
-
-    def row_hop(a, kind, k, i):
+            shards_in[a] if first else block, block, *sems, x_peer if kind == 1 else core_peer
+        )
+
+    def row_hop(a, kind, k):
+        i = behind(k)
+        sems = (send_rows.at[a, kind, k], recv_rows.at[a, kind, k])
         if kind == 0:
-            return copy_to(
-                rows_in[a].at[ahead(k)],
-                row_slice(a, me, t),
-                send_rows.at[a, 0, k],
-                recv_rows.at[a, 0, k],
-                (ahead(k), t),
-            )
-        if kind == 3:
-            return copy_to(
-                row_slice(a, i, t_x),
-                row_slice(a, i, t_x),
-                send_rows.at[a, 3, k],
-                recv_rows.at[a, 3, k],
-                core_peer,
-            )
-        return copy_to(
-            row_slice(a, i, t),
-            row_slice(a, i, t),
-            send_rows.at[a, kind, k],
-            recv_rows.at[a, kind, k],
-            x_peer if kind == 1 else core_peer,
-        )
+            return copy_to(rows_in[a].at[ahead(k)], row_slice(a, me, t), *sems, (ahead(k), t))
+        block = row_slice(a, i, t_x if kind == 3 else t)
+        return copy_to(block, block, *sems, x_peer if kind == 1 else core_peer)
 
     def w_hop(k):
         return copy_to(
-            weight_rows.at[ahead(k)],
-            weight_all.at[me],
-            send_w.at[k],
-            recv_w.at[k],
-            (ahead(k), t),
+            weight_rows.at[ahead(k)], weight_all.at[me], send_w.at[k], recv_w.at[k], (ahead(k), t)
         )
 
     for a in range(2):
-        go(shard_hop(a, 1, 0, me, True))
-        go(shard_hop(a, 2, 0, me, True))
-    for k in range(1, n_ep):
+        shard_hop(a, 1, 0, True).start()
+        shard_hop(a, 2, 0, True).start()
+
+    @pl.loop(1, n_ep)
+    def _(k):
         for a in range(2):
-            go(shard_hop(a, 0, k, me))
-        go(w_hop(k))
+            shard_hop(a, 0, k).start()
+        w_hop(k).start()
         for a in range(2):
-            go(row_hop(a, 0, k, me))
+            row_hop(a, 0, k).start()
 
     ins = [
-        pltpu.make_async_copy(x_own, own_buf.at[0], local_sem.at[0]),
-        pltpu.make_async_copy(dy_own, own_buf.at[1], local_sem.at[1]),
-        pltpu.make_async_copy(in_own, shard_buf.at[0], local_sem.at[2]),
-        pltpu.make_async_copy(out_own, shard_buf.at[1], local_sem.at[3]),
+        pltpu.make_async_copy(in_own, shard_buf.at[0], local_sem.at[0]),
+        pltpu.make_async_copy(out_own, shard_buf.at[1], local_sem.at[1]),
+        pltpu.make_async_copy(x_own, x_all.at[me], local_sem.at[2]),
+        pltpu.make_async_copy(dy_own, dy_all.at[me], local_sem.at[3]),
     ]
     outs = [
-        pltpu.make_async_copy(own_buf.at[0], x_all.at[me], local_sem.at[4]),
-        pltpu.make_async_copy(own_buf.at[1], dy_all.at[me], local_sem.at[5]),
-        pltpu.make_async_copy(shard_buf.at[0], in_all.at[me, t], local_sem.at[6]),
-        pltpu.make_async_copy(shard_buf.at[1], out_all.at[me, t], local_sem.at[7]),
+        pltpu.make_async_copy(shard_buf.at[0], in_all.at[me, t], local_sem.at[4]),
+        pltpu.make_async_copy(shard_buf.at[1], out_all.at[me, t], local_sem.at[5]),
     ]
     for c in ins:
         c.start()
     weight_all[pl.ds(me, 1)] = weight_rows[pl.ds(me, 1)]
-    for c, o in zip(ins, outs):
+    for c in ins:
         c.wait()
-        o.start()
-
-    def relay(k):
-        i = behind(k)
-        for a in range(2):
-            shard_hop(a, 1, k, i).wait_recv()
-            go(shard_hop(a, 3, k, i))
-            if k > 0:
-                row_hop(a, 1, k, i).wait_recv()
-                go(row_hop(a, 3, k, i))
-
-    for k in range(1, n_ep):
-        i = behind(k)
-        for a in range(2):
-            shard_hop(a, 0, k, i).wait_recv()
-            go(shard_hop(a, 1, k, i))
-            go(shard_hop(a, 2, k, i))
-            row_hop(a, 0, k, i).wait_recv()
-            go(row_hop(a, 1, k, i))
-            go(row_hop(a, 2, k, i))
-        relay(k - 1)
-    relay(n_ep - 1)
-
-    for k in range(n_ep):
-        i = behind(k)
+    for c in outs:
+        c.start()
+
+    diagonal = lax.broadcasted_iota(jnp.int32, (cap, lanes), 0) == lax.broadcasted_iota(
+        jnp.int32, (cap, lanes), 1
+    )
+    contract_cols = (((1,), (1,)), ((), ()))
+
+    def compute(i):
+        weight_row = weight_all[i, 0:1].astype(f32)
+        route_col = jnp.sum(jnp.where(diagonal, weight_row, 0.0), axis=1, keepdims=True)
+        x_rows = x_all[i]
+        gate_pre = jnp.dot(x_rows, gate_w[...], preferred_element_type=f32)
+        up_pre = jnp.dot(x_rows, up_w[...], preferred_element_type=f32)
+        gate_clamp = jnp.minimum(gate_pre, CLAMP_LIMIT)
+        up_clamp = jnp.clip(up_pre, -CLAMP_LIMIT, CLAMP_LIMIT)
+        sig = jax.nn.sigmoid(SIG_SLOPE * gate_clamp)
+        act = (gate_clamp * sig * (up_clamp + 1.0)).astype(bf)
+        act_all[i] = act
+        dy_rows = dy_all[i]
+        scaled_all[i] = (route_col * dy_rows.astype(f32)).astype(bf)
+        back = lax.dot_general(
+            dy_rows, down_w[...], contract_cols, preferred_element_type=f32
+        )
+        weight_sum = jnp.sum(act.astype(f32) * back, axis=1, keepdims=True)
+        weight_lane = jnp.sum(jnp.where(diagonal, weight_sum, 0.0), axis=0, keepdims=True)
+        weight_part[i] = jnp.broadcast_to(weight_lane, (8, lanes))
+        d_act = route_col * back
+        d_gate = jnp.where(
+            gate_pre < CLAMP_LIMIT,
+            d_act * (up_clamp + 1.0) * (sig + SIG_SLOPE * gate_clamp * sig * (1.0 - sig)),
+            0.0,
+        ).astype(bf)
+        d_up = jnp.where(jnp.abs(up_pre) < CLAMP_LIMIT, d_act * gate_clamp * sig, 0.0).astype(bf)
+        dgate_all[i] = d_gate
+        dup_all[i] = d_up
+        part = lax.dot_general(d_gate, gate_w[...], contract_cols, preferred_element_type=f32)
+        part = part + lax.dot_general(d_up, up_w[...], contract_cols, preferred_element_type=f32)
+        part_all[i] = part.astype(bf)
+
+    @pl.loop(0, n_ep + 2)
+    def _(n):
+        @pl.when((n >= 1) & (n < n_ep))
+        def _():
+            for a in range(2):
+                shard_hop(a, 0, n).wait_recv()
+                shard_hop(a, 1, n).start()
+                shard_hop(a, 2, n).start()
+            for a in range(2):
+                row_hop(a, 0, n).wait_recv()
+                row_hop(a, 1, n).start()
+                row_hop(a, 2, n).start()
+
+        @pl.when((n >= 1) & (n < n_ep + 1))
+        def _():
+            k = n - 1
+            for a in range(2):
+                shard_hop(a, 1, k).wait_recv()
+                shard_hop(a, 3, k).start()
+
+        @pl.when((n >= 2) & (n < n_ep + 1))
+        def _():
+            k = n - 1
+            for a in range(2):
+                row_hop(a, 1, k).wait_recv()
+                row_hop(a, 3, k).start()
+
+        @pl.when(n >= 3)
+        def _():
+            k = n - 2
+            w_hop(k).wait_recv()
+            for a in range(2):
+                for kind in (2, 3):
+                    row_hop(a, kind, k).wait_recv()
+
+        @pl.when((n == 0) | (n >= 3))
+        def _():
+            compute(behind(jnp.maximum(n - 2, 0)))
+
+    @pl.loop(0, n_ep)
+    def _(k):
         for a in range(2):
             for kind in (2, 3):
-                shard_hop(a, kind, k, i).wait_recv()
-                if k > 0:
-                    row_hop(a, kind, k, i).wait_recv()
-        if k > 0:
-            w_hop(k).wait_recv()
-    for c in started:
-        c.wait_send()
-    for o in outs:
-        o.wait()
+                shard_hop(a, kind, k).wait_recv()
+            for kind in (1, 2, 3):
+                shard_hop(a, kind, k).wait_send()
+
+    @pl.loop(1, n_ep)
+    def _(k):
+        for a in range(2):
+            shard_hop(a, 0, k).wait_send()
+            for kind in range(4):
+                row_hop(a, kind, k).wait_send()
+        w_hop(k).wait_send()
+
+    for c in outs:
+        c.wait()
 
 
 def return_kernel(
@@ -383,28 +406,36 @@
 
 
 def dispatch(n_ep, n_tp, *args):
-    x_quarter, dy_quarter, x_own, dy_own, weight_rows, in_own, out_own = args
+    x_quarter, _, x_own, _, weight_rows, in_own, _, gate_w, _, _ = args
     cap, cols = x_quarter.shape[1:]
     width = x_own.shape[1]
+    hidden = gate_w.shape[1]
+    lanes = weight_rows.shape[2]
     bf = jnp.bfloat16
     dma = pltpu.SemaphoreType.DMA
     rows = jax.ShapeDtypeStruct((n_ep, cap, width), bf)
+    inner = jax.ShapeDtypeStruct((n_ep, cap, hidden), bf)
     shard = jax.ShapeDtypeStruct((n_ep, n_tp) + in_own.shape, bf)
     return pl.pallas_call(
         functools.partial(dispatch_kernel, n_ep),
         out_shape=(
             rows,
             rows,
-            jax.ShapeDtypeStruct(weight_rows.shape, weight_rows.dtype),
+            inner,
+            inner,
+            inner,
+            rows,
+            jax.ShapeDtypeStruct((n_ep, 8, lanes), jnp.float32),
             shard,
             shard,
         ),
-        in_specs=[ANY, ANY, ANY, ANY, VMEM, ANY, ANY],
-        out_specs=(ANY, ANY, VMEM, ANY, ANY),
+        in_specs=[ANY, ANY, ANY, ANY, VMEM, ANY, ANY, VMEM, VMEM, VMEM],
+        out_specs=(VMEM,) * 7 + (ANY, ANY),
         scratch_shapes=[
-            pltpu.VMEM((2, cap, width), bf),
+            pltpu.VMEM((n_ep, cap, width), bf),
+            pltpu.VMEM(weight_rows.shape, bf),
             pltpu.VMEM((2,) + in_own.shape, bf),
-            dma((8,)),
+            dma((6,)),
             dma((2, 4, n_ep)),
             dma((2, 4, n_ep)),
             dma((2, 4, n_ep)),
@@ -412,7 +443,9 @@
             dma((n_ep,)),
             dma((n_ep,)),
         ],
-        compiler_params=pltpu.CompilerParams(collective_id=0, has_side_effects=True),
+        compiler_params=pltpu.CompilerParams(
+            collective_id=0, has_side_effects=True, vmem_limit_bytes=56 * 1024 * 1024
+        ),
         name="dispatch",
     )(*args)
 
@@ -513,48 +546,30 @@
     weight_rows = jnp.broadcast_to(
         weight_rows.reshape(count_ep, 1, lanes), (count_ep, 16, lanes)
     )
-    x_in, dy_in, weight_in, in_all, out_all = dispatch(
-        count_ep, count_tp, x_quarter, dy_quarter, x_own, dy_own, weight_rows, dense_in, dense_out
+    x_in, scaled_in, act, d_gate, d_up, part, weight_part, in_all, out_all = dispatch(
+        count_ep,
+        count_tp,
+        x_quarter,
+        dy_quarter,
+        x_own,
+        dy_own,
+        weight_rows,
+        dense_in,
+        dense_out,
+        w_gate[0],
+        w_up[0],
+        w_down[0],
     )
     in_whole = in_all.reshape(model_width, -1)
     out_whole = out_all.reshape(model_width, -1)
-
     x_slots = x_in.reshape(slot_total, model_width)
-    dy_slots = dy_in.reshape(slot_total, model_width)
-    route_col = weight_in[:, 0, :capacity].reshape(slot_total, 1).astype(f32)
-    gate_w = w_gate[0]
-    up_w = w_up[0]
-    down_w = w_down[0]
-    gate_pre = jnp.dot(x_slots, gate_w, preferred_element_type=f32)
-    up_pre = jnp.dot(x_slots, up_w, preferred_element_type=f32)
-    gate_clamp = jnp.minimum(gate_pre, CLAMP_LIMIT)
-    up_clamp = jnp.clip(up_pre, -CLAMP_LIMIT, CLAMP_LIMIT)
-    sig = jax.nn.sigmoid(SIG_SLOPE * gate_clamp)
-    act = (gate_clamp * sig * (up_clamp + 1.0)).astype(bf)
-    back = lax.dot_general(
-        dy_slots, down_w, (((1,), (1,)), ((), ())), preferred_element_type=f32
-    )
-    d_act = route_col * back
-    d_gate = jnp.where(
-        gate_pre < CLAMP_LIMIT,
-        d_act * (up_clamp + 1.0) * (sig + SIG_SLOPE * gate_clamp * sig * (1.0 - sig)),
-        0.0,
-    ).astype(bf)
-    d_up = jnp.where(jnp.abs(up_pre) < CLAMP_LIMIT, d_act * gate_clamp * sig, 0.0).astype(bf)
-    scaled_cot = (route_col * dy_slots.astype(f32)).astype(bf)
+    scaled_cot = scaled_in.reshape(slot_total, model_width)
     contract_rows = (((0,), (0,)), ((), ()))
+    contract_cols = (((1,), (1,)), ((), ()))
+    act, d_gate, d_up = (a.reshape(slot_total, -1) for a in (act, d_gate, d_up))
     grad_gate = lax.dot_general(x_slots, d_gate, contract_rows, preferred_element_type=f32)
     grad_up = lax.dot_general(x_slots, d_up, contract_rows, preferred_element_type=f32)
     grad_down = lax.dot_general(act, scaled_cot, contract_rows, preferred_element_type=f32)
-    contract_cols = (((1,), (1,)), ((), ()))
-    row_partial = lax.dot_general(d_gate, gate_w, contract_cols, preferred_element_type=f32)
-    row_partial = row_partial + lax.dot_general(
-        d_up, up_w, contract_cols, preferred_element_type=f32
-    )
-    part = row_partial.astype(bf).reshape(count_ep, capacity, model_width)
-    weight_part = jnp.sum(act.astype(f32) * back, axis=1).reshape(count_ep, capacity)
-    weight_part = jnp.pad(weight_part, ((0, 0), (0, lanes - capacity)))
-    weight_part = jnp.broadcast_to(weight_part[:, None, :], (count_ep, 8, lanes))
 
     dense_pre = jnp.dot(tokens, in_whole, preferred_element_type=f32)
     dense_act = jax.nn.silu(dense_pre).astype(bf)
@@ -588,13 +603,13 @@
         count_ep,
         count_tp,
         part,
-        in_partial.reshape(count_ep, block_cols, -1),
-        out_partial.reshape(count_ep, block_cols, -1),
+        in_partial.astype(bf).reshape(count_ep, block_cols, -1),
+        out_partial.astype(bf).reshape(count_ep, block_cols, -1),
         gate_partial,
         weight_part,
     )
-    grad_dense_in = jnp.sum(in_back, axis=0)
-    grad_dense_out = jnp.sum(out_back, axis=0)
+    grad_dense_in = jnp.sum(in_back.astype(f32), axis=0)
+    grad_dense_out = jnp.sum(out_back.astype(f32), axis=0)
     grad_dense_gate = jnp.sum(gate_back[:, 0, :block_cols], axis=0)
     expert_dx = lax.dot_general(
         pick, rows_back.reshape(slot_total, col_count), contract_rows, preferred_element_type=f32

time: 267 us -> 224 us (0.84)
  matrix products: 71.3 us -> 32 us
    dot_general x5 -> x0, matrix products: 29.1 us -> none  [the longest x1 9.69 us: shards(): lax.dot_general(dy_slots, down_w, (((1,), (1,)), ((), ())), preferred_ele...]
    pallas_call x1, Pallas kernels: 93.9 us -> 105 us  [dispatch(): pl.pallas_call(functools.partial(dispatch_kernel, n_ep), out_shape=(rows,...]
    pallas_call x1, Pallas kernels: 80.6 us -> 70.3 us  [give_back(): pl.pallas_call(functools.partial(return_kernel, n_ep, n_tp), out_shape=(j...]
    dot_general x1, matrix products: 7.94 us -> 4.46 us  [shards(): lax.dot_general(x_slots, d_up, contract_rows, preferred_element_type=f32)]
    dot_general x1, matrix products: 7.18 us -> 4.44 us  [shards(): lax.dot_general(x_slots, d_gate, contract_rows, preferred_element_type=f32)]
where the time goes in v2:
time: 224 us; the launch traced here: 223 us
  Pallas kernels  175 us (78%)
  matrix products  32 us (14%)
  other arithmetic  8.67 us (4%)
  local copies, waits for them, and re-layouts  6.66 us (3%)
    pallas_call x1, Pallas kernels, dispatch(): pl.pallas_call(functools.partial(dispatch_kernel, n_ep), out_shape=(rows,...  105 us
    pallas_call x1, Pallas kernels, give_back(): pl.pallas_call(functools.partial(return_kernel, n_ep, n_tp), out_shape=(j...  70.3 us
    dot_general x1, matrix products, shards(): lax.dot_general(act, scaled_cot, contract_rows, preferred_element_type=f32)  7.34 us

profile of v2, /device:TPU:13, one launch (start us, length us, event | category | flops | bytes accessed | tf_op | source)
XLA Modules:
  0.0 223.5 jit_solution(10207559120306884221)
XLA Ops:
  0.6 0.0 copy-start.2
  0.6 0.8 fusion.16
  1.4 0.1 fusion.6
  1.6 0.8 select_reduce_fusion.2
  2.3 0.7 multiply_add_fusion
  3.1 2.9 %fusion.7 = bf16[1280,512]{1,0:T(8,128)(2,1)} fusion(bf16[320,2048]{1,0:T(8,128)(2,1)} %param.11, s32[]{:T(128)S(6)} %select_n.27, s32[320]{0:T(512)S(1)} %get-tuple-element.37, s32[320]{0:T(512)S(1)} %get-tuple-element.36), kind=kOutput, calls=%fused_computation.30 | convolution fusion | flops 420659200 | bytes 1640964 | tf_op jit(solution)/shard_map/dot_general | solution.py:537
  6.0 0.0 copy-done.2
  6.0 1.9 fusion.9
  7.9 0.4 fusion.1
  8.3 0.0 copy-done.3
  8.3 0.0 copy-start.6
  8.3 1.4 fusion.12.dy_own
  9.7 1.3 fusion.14.x_own
  11.0 0.0 copy-done.6
  11.0 0.7 select_reduce_fusion.1
  11.8 0.6 broadcast_in_dim.68.weight_rows
  12.4 104.9 %dispatch.1 = (bf16[8,160,2048]{2,1,0:T(8,128)(2,1)}, bf16[8,160,2048]{2,1,0:T(8,128)(2,1)}, bf16[8,160,512]{2,1,0:T(8,128)(2,1)}, bf16[8,160,512]{2,1,0:T(8,128...) custom-call(bf16[8,160,512]{2,1,0:T(8,128)(2,1)} %bitcast.59, ...), custom_call_target="tpu_custom_call" | custom-call | tf_op jit(solution)/shard_map/dispatch/pallas_call | solution.py:419
  117.4 0.0 copy-start.10
  117.4 1.8 convolution_bitcast_fusion.3
  119.2 0.0 copy-done.10
  119.2 0.0 copy-start.5
  119.2 0.7 fusion.2
  119.9 0.0 copy-done.5
  119.9 0.5 convolution_reduce_fusion
  120.4 1.3 fusion
  121.7 1.8 copy.29
  123.6 0.1 constant_dynamic-slice_fusion
  123.6 0.4 convolution_convert_fusion
  124.0 0.0 copy-start.4
  124.0 1.6 copy.28
  125.6 1.2 multiply_reduce_fusion
  126.7 0.0 copy-done.4
  126.7 0.0 copy-start.1
  126.7 1.8 fusion.5
  128.5 0.3 convolution_convert_fusion.1
  128.9 2.5 %copy-done = bf16[8,160,2048]{2,1,0:T(8,128)(2,1)S(1)} copy-done((bf16[8,160,2048]{2,1,0:T(8,128)(2,1)S(1)}, bf16[8,160,2048]{2,1,0:T(8,128)(2,1)}, u32[]{:S(2)}) %copy-start) | copy-done | bytes 5242904
  131.3 70.3 %give_back.1 = (bf16[8,160,512]{2,1,0:T(8,128)(2,1)S(1)}, bf16[8,64,256]{2,1,0:T(8,128)(2,1)S(1)}, bf16[8,64,256]{2,1,0:T(8,128)(2,1)S(1)}, f32[8,8,128]{2,1,0:T(8,128)S(1)}, f32[8,4,8,256]{3,2,1,0:T(8,128)S(1)}) custom-call(bf16[8,160,2048]{2,1,0:T(8,128)(2,1)S(1)} %copy-done, bf16[8,64,256]{2,1,0:T(8,128)(2,1)S(1)} %bitcast.49, ...), custom_call_target="tpu_custom_call" | custom-call | tf_op jit(solution)/shard_map/give_back/pallas_call | solution.py:460
  201.7 0.0 slice-start
  201.7 0.7 convert_reduce_fusion
  202.4 7.3 %convolution_bitcast_fusion = f32[1,512,2048]{2,1,0:T(8,128)} fusion(bf16[8,160,512]{2,1,0:T(8,128)(2,1)S(1)} %copy-done.9, bf16[8,160,2048]{2,1,0:T(8,128)(2,1)} %get-tuple-element.32), kind=kOutput, calls=%fused_computation.5 | convolution fusion | flops 2684354560 | bytes 10747904 | tf_op jit(solution)/shard_map/dot_general | solution.py:572
  209.7 0.0 slice-done.1
  209.8 4.5 %convolution_bitcast_fusion.1 = f32[1,2048,512]{2,1,0:T(8,128)} fusion(bf16[8,160,2048]{2,1,0:T(8,128)(2,1)S(1)} %bitcast.67, bf16[8,160,512]{2,1,0:T(8,128)(2,1)S(1)} %copy-done.8), kind=kOutput, calls=%fused_computation.6 | convolution fusion | flops 2684354560 | bytes 10747904 | tf_op jit(solution)/shard_map/dot_general | solution.py:571
  214.2 4.4 %convolution_bitcast_fusion.2 = f32[1,2048,512]{2,1,0:T(8,128)} fusion(bf16[8,160,2048]{2,1,0:T(8,128)(2,1)S(1)} %bitcast.67, bf16[8,160,512]{2,1,0:T(8,128)(2,1)S(1)} %copy-done.7), kind=kOutput, calls=%fused_computation.7 | convolution fusion | flops 2684354560 | bytes 10747904 | tf_op jit(solution)/shard_map/dot_general | solution.py:570
  218.7 0.1 dynamic-slice_convert_fusion
  218.8 1.2 convolution_add_fusion.1
  220.0 1.5 fusion.3
  221.6 1.4 select_reduce_fusion
  222.9 0.5 slice_reduce_fusion.1
  (20 shorter events, 0.1 us)
Async XLA Ops:
  0.6 5.3 %copy-start.2 = (bf16[320,2048]{1,0:T(8,128)(2,1)S(1)}, bf16[320,2048]{1,0:T(8,128)(2,1)}, u32[]{:S(2)}) copy-start(bf16[320,2048]{1,0:T(8,128)(2,1)} %param.10) | copy-start | bytes 3932164
  6.0 2.3 %copy-start.3 = (bf16[320,2048]{1,0:T(8,128)(2,1)S(1)}, bf16[320,2048]{1,0:T(8,128)(2,1)}, u32[]{:S(2)}) copy-start(bf16[320,2048]{1,0:T(8,128)(2,1)} %param.11) | copy-start | bytes 3932164
  8.3 2.7 %copy-start.6 = (bf16[320,2]{0,1:T(2,128)(2,1)S(1)}, bf16[320,2]{0,1:T(2,128)(2,1)}, u32[]{:S(2)}) copy-start(bf16[320,2]{0,1:T(2,128)(2,1)} %param.13) | copy-start | bytes 3844
  117.4 1.8 copy-start.10
  119.2 0.7 copy-start.5
  124.0 2.7 %copy-start.4 = (bf16[320,2048]{1,0:T(8,128)(2,1)S(1)}, bf16[320,2048]{1,0:T(8,128)(2,1)}, u32[]{:S(2)}) copy-start(bf16[320,2048]{1,0:T(8,128)(2,1)} %fusion) | copy-start | bytes 3932164
  126.7 2.1 copy-start.1
  128.8 2.5 %copy-start = (bf16[8,160,2048]{2,1,0:T(8,128)(2,1)S(1)}, bf16[8,160,2048]{2,1,0:T(8,128)(2,1)}, u32[]{:S(2)}) copy-start(bf16[8,160,2048]{2,1,0:T(8,128)(2,1)} %get-tuple-element.24.part) | copy-start | bytes 15728644
  131.3 71.1 %copy-start.9 = (bf16[8,160,512]{2,1,0:T(8,128)(2,1)S(1)}, bf16[8,160,512]{2,1,0:T(8,128)(2,1)}, u32[]{:S(2)}) copy-start(bf16[8,160,512]{2,1,0:T(8,128)(2,1)} %get-tuple-element.31) | copy-start | bytes 3932164
  201.7 8.1 %slice-start = ((s8[5242880]{0:T(1024)(128)(4,1)}), s8[4194304]{0:T(1024)(128)(4,1)S(1)}, s32[]{:S(2)}) async-start(s8[5242880]{0:T(1024)(128)(4,1)} %bitcast.66), calls=%async_computation | async-start | bytes 8388608
  202.4 7.3 %slice-start.1 = ((s8[5242880]{0:T(1024)(128)(4,1)}), s8[1048576]{0:T(1024)(128)(4,1)S(1)}, s32[]{:S(2)}) async-start(s8[5242880]{0:T(1024)(128)(4,1)} %bitcast.66), calls=%async_computation.1 | async-start | bytes 2097152
  202.4 7.4 %copy-start.8 = (bf16[8,160,512]{2,1,0:T(8,128)(2,1)S(1)}, bf16[8,160,512]{2,1,0:T(8,128)(2,1)}, u32[]{:S(2)}) copy-start(bf16[8,160,512]{2,1,0:T(8,128)(2,1)} %get-tuple-element.30) | copy-start | bytes 3932164
  209.8 4.5 %copy-start.7 = (bf16[8,160,512]{2,1,0:T(8,128)(2,1)S(1)}, bf16[8,160,512]{2,1,0:T(8,128)(2,1)}, u32[]{:S(2)}) copy-start(bf16[8,160,512]{2,1,0:T(8,128)(2,1)} %get-tuple-element.29) | copy-start | bytes 3932164

commit v3 on v2

--- a/solution.py
+++ b/solution.py
@@ -33,19 +33,26 @@
     gate_w,
     up_w,
     down_w,
+    x_out,
+    scaled_out,
+    act_out,
+    dgate_out,
+    dup_out,
+    part_out,
+    weight_part,
+    in_all,
+    out_all,
     x_all,
     scaled_all,
     act_all,
     dgate_all,
     dup_all,
     part_all,
-    weight_part,
-    in_all,
-    out_all,
     dy_all,
     weight_all,
     shard_buf,
     local_sem,
+    out_sem,
     send_rows,
     recv_rows,
     send_shard,
@@ -70,6 +77,9 @@
     def behind(k):
         return lax.rem(me + n_ep - k, n_ep)
 
+    def offset(n):
+        return n_ep // 2 + (n // 2) * (1 - 2 * (n % 2))
+
     core_peer = (me, t_core)
     x_peer = (me, t_x)
     greet([(ahead(k), t) for k in range(1, n_ep)] + [core_peer, x_peer])
@@ -123,7 +133,8 @@
         shard_hop(a, 2, 0, True).start()
 
     @pl.loop(1, n_ep)
-    def _(k):
+    def _(n):
+        k = offset(n)
         for a in range(2):
             shard_hop(a, 0, k).start()
         w_hop(k).start()
@@ -185,36 +196,52 @@
         part = part + lax.dot_general(d_up, up_w[...], contract_cols, preferred_element_type=f32)
         part_all[i] = part.astype(bf)
 
+    results = (
+        (x_all, x_out),
+        (part_all, part_out),
+        (scaled_all, scaled_out),
+        (act_all, act_out),
+        (dgate_all, dgate_out),
+        (dup_all, dup_out),
+    )
+
+    def store(i):
+        return [
+            pltpu.make_async_copy(src.at[i], dst.at[i], out_sem.at[a, i])
+            for a, (src, dst) in enumerate(results)
+        ]
+
     @pl.loop(0, n_ep + 2)
     def _(n):
         @pl.when((n >= 1) & (n < n_ep))
         def _():
+            k = offset(n)
             for a in range(2):
-                shard_hop(a, 0, n).wait_recv()
-                shard_hop(a, 1, n).start()
-                shard_hop(a, 2, n).start()
+                shard_hop(a, 0, k).wait_recv()
+                shard_hop(a, 1, k).start()
+                shard_hop(a, 2, k).start()
             for a in range(2):
-                row_hop(a, 0, n).wait_recv()
-                row_hop(a, 1, n).start()
-                row_hop(a, 2, n).start()
+                row_hop(a, 0, k).wait_recv()
+                row_hop(a, 1, k).start()
+                row_hop(a, 2, k).start()
 
         @pl.when((n >= 1) & (n < n_ep + 1))
         def _():
-            k = n - 1
+            k = jnp.where(n == 1, 0, offset(jnp.maximum(n - 1, 1)))
             for a in range(2):
                 shard_hop(a, 1, k).wait_recv()
                 shard_hop(a, 3, k).start()
 
         @pl.when((n >= 2) & (n < n_ep + 1))
         def _():
-            k = n - 1
+            k = offset(n - 1)
             for a in range(2):
                 row_hop(a, 1, k).wait_recv()
                 row_hop(a, 3, k).start()
 
         @pl.when(n >= 3)
         def _():
-            k = n - 2
+            k = offset(n - 2)
             w_hop(k).wait_recv()
             for a in range(2):
                 for kind in (2, 3):
@@ -222,7 +249,10 @@
 
         @pl.when((n == 0) | (n >= 3))
         def _():
-            compute(behind(jnp.maximum(n - 2, 0)))
+            i = behind(jnp.where(n == 0, 0, offset(jnp.maximum(n - 2, 1))))
+            compute(i)
+            for c in store(i):
+                c.start()
 
     @pl.loop(0, n_ep)
     def _(k):
@@ -231,6 +261,8 @@
                 shard_hop(a, kind, k).wait_recv()
             for kind in (1, 2, 3):
                 shard_hop(a, kind, k).wait_send()
+        for c in store(k):
+            c.wait()
 
     @pl.loop(1, n_ep)
     def _(k):
@@ -430,12 +462,19 @@
             shard,
         ),
         in_specs=[ANY, ANY, ANY, ANY, VMEM, ANY, ANY, VMEM, VMEM, VMEM],
-        out_specs=(VMEM,) * 7 + (ANY, ANY),
+        out_specs=(ANY,) * 6 + (VMEM, ANY, ANY),
         scratch_shapes=[
-            pltpu.VMEM((n_ep, cap, width), bf),
+            pltpu.VMEM(rows.shape, bf),
+            pltpu.VMEM(rows.shape, bf),
+            pltpu.VMEM(inner.shape, bf),
+            pltpu.VMEM(inner.shape, bf),
+            pltpu.VMEM(inner.shape, bf),
+            pltpu.VMEM(rows.shape, bf),
+            pltpu.VMEM(rows.shape, bf),
             pltpu.VMEM(weight_rows.shape, bf),
             pltpu.VMEM((2,) + in_own.shape, bf),
             dma((6,)),
+            dma((6, n_ep)),
             dma((2, 4, n_ep)),
             dma((2, 4, n_ep)),
             dma((2, 4, n_ep)),

time: 224 us -> 220 us (0.982)
  Pallas kernels: 175 us -> 171 us
    pallas_call x1, Pallas kernels: 70.3 us -> 53.8 us  [give_back(): pl.pallas_call(functools.partial(return_kernel, n_ep, n_tp), out_shape=(j...]
    pallas_call x1, Pallas kernels: 105 us -> 117 us  [dispatch(): pl.pallas_call(functools.partial(dispatch_kernel, n_ep), out_shape=(rows,...]
where the time goes in v3:
time: 220 us; the launch traced here: 219 us
  Pallas kernels  171 us (78%)
  matrix products  32 us (15%)
  other arithmetic  8.67 us (4%)
  local copies, waits for them, and re-layouts  6.67 us (3%)
    pallas_call x1, Pallas kernels, dispatch(): pl.pallas_call(functools.partial(dispatch_kernel, n_ep), out_shape=(rows,...  117 us
    pallas_call x1, Pallas kernels, give_back(): pl.pallas_call(functools.partial(return_kernel, n_ep, n_tp), out_shape=(j...  53.8 us
    dot_general x1, matrix products, shards(): lax.dot_general(act, scaled_cot, contract_rows, preferred_element_type=f32)  7.34 us
    dot_general x1, matrix products, shards(): lax.dot_general(x_slots, d_up, contract_rows, preferred_element_type=f32)  4.45 us
    dot_general x1, matrix products, shards(): lax.dot_general(x_slots, d_gate, contract_rows, preferred_element_type=f32)  4.43 us

profile of v3, /device:TPU:13, one launch (start us, length us, event | category | flops | bytes accessed | tf_op | source)
XLA Modules:
  0.0 219.0 jit_solution(14443682918779645805)
XLA Ops:
  0.6 0.0 copy-start.2
  0.6 0.8 fusion.16
  1.4 0.1 fusion.6
  1.6 0.8 select_reduce_fusion.2
  2.3 0.7 multiply_add_fusion
  3.1 2.9 %fusion.7 = bf16[1280,512]{1,0:T(8,128)(2,1)} fusion(bf16[320,2048]{1,0:T(8,128)(2,1)} %param.11, s32[]{:T(128)S(6)} %select_n.27, s32[320]{0:T(512)S(1)} %get-tuple-element.37, s32[320]{0:T(512)S(1)} %get-tuple-element.36), kind=kOutput, calls=%fused_computation.30 | convolution fusion | flops 420659200 | bytes 1640964 | tf_op jit(solution)/shard_map/dot_general | solution.py:576
  6.0 0.0 copy-done.2
  6.0 1.9 fusion.9
  7.9 0.4 fusion.1
  8.3 0.0 copy-done.3
  8.3 0.0 copy-start.6
  8.3 1.4 fusion.12.dy_own
  9.7 1.3 fusion.14.x_own
  11.0 0.0 copy-done.6
  11.0 0.7 select_reduce_fusion.1
  11.8 0.6 broadcast_in_dim.68.weight_rows
  12.4 117.1 %dispatch.1 = (bf16[8,160,2048]{2,1,0:T(8,128)(2,1)}, bf16[8,160,2048]{2,1,0:T(8,128)(2,1)}, bf16[8,160,512]{2,1,0:T(8,128)(2,1)}, bf16[8,160,512]{2,1,0:T(8,128...) custom-call(bf16[8,160,512]{2,1,0:T(8,128)(2,1)} %bitcast.59, ...), custom_call_target="tpu_custom_call" | custom-call | tf_op jit(solution)/shard_map/dispatch/pallas_call | solution.py:451
  129.5 0.0 copy-start.10
  129.5 1.8 convolution_bitcast_fusion.3
  131.4 0.0 copy-done.10
  131.4 0.0 copy-start.5
  131.4 0.7 fusion.2
  132.0 0.0 copy-done.5
  132.1 0.5 convolution_reduce_fusion
  132.6 1.3 fusion
  133.9 1.8 copy.29
  135.7 0.1 constant_dynamic-slice_fusion
  135.8 0.4 convolution_convert_fusion
  136.2 0.0 copy-start.4
  136.2 1.6 copy.28
  137.7 1.2 multiply_reduce_fusion
  138.9 0.0 copy-done.4
  138.9 0.0 copy-start.1
  138.9 1.8 fusion.5
  140.7 0.3 convolution_convert_fusion.1
  141.0 2.5 %copy-done = bf16[8,160,2048]{2,1,0:T(8,128)(2,1)S(1)} copy-done((bf16[8,160,2048]{2,1,0:T(8,128)(2,1)S(1)}, bf16[8,160,2048]{2,1,0:T(8,128)(2,1)}, u32[]{:S(2)}) %copy-start) | copy-done | bytes 5242904
  143.5 53.8 %give_back.1 = (bf16[8,160,512]{2,1,0:T(8,128)(2,1)S(1)}, bf16[8,64,256]{2,1,0:T(8,128)(2,1)S(1)}, bf16[8,64,256]{2,1,0:T(8,128)(2,1)S(1)}, f32[8,8,128]{2,1,0:T(8,128)S(1)}, f32[8,4,8,256]{3,2,1,0:T(8,128)S(1)}) custom-call(bf16[8,160,2048]{2,1,0:T(8,128)(2,1)S(1)} %copy-done, bf16[8,64,256]{2,1,0:T(8,128)(2,1)S(1)} %bitcast.49, ...), custom_call_target="tpu_custom_call" | custom-call | tf_op jit(solution)/shard_map/give_back/pallas_call | solution.py:499
  197.3 0.0 slice-start
  197.3 0.7 convert_reduce_fusion
  198.0 7.3 %convolution_bitcast_fusion = f32[1,512,2048]{2,1,0:T(8,128)} fusion(bf16[8,160,512]{2,1,0:T(8,128)(2,1)S(1)} %copy-done.9, bf16[8,160,2048]{2,1,0:T(8,128)(2,1)} %get-tuple-element.32), kind=kOutput, calls=%fused_computation.5 | convolution fusion | flops 2684354560 | bytes 10747904 | tf_op jit(solution)/shard_map/dot_general | solution.py:611
  205.4 0.0 copy-done.8
  205.4 4.5 %convolution_bitcast_fusion.1 = f32[1,2048,512]{2,1,0:T(8,128)} fusion(bf16[8,160,2048]{2,1,0:T(8,128)(2,1)S(1)} %bitcast.67, bf16[8,160,512]{2,1,0:T(8,128)(2,1)S(1)} %copy-done.8), kind=kOutput, calls=%fused_computation.6 | convolution fusion | flops 2684354560 | bytes 10747904 | tf_op jit(solution)/shard_map/dot_general | solution.py:610
  209.8 4.4 %convolution_bitcast_fusion.2 = f32[1,2048,512]{2,1,0:T(8,128)} fusion(bf16[8,160,2048]{2,1,0:T(8,128)(2,1)S(1)} %bitcast.67, bf16[8,160,512]{2,1,0:T(8,128)(2,1)S(1)} %copy-done.7), kind=kOutput, calls=%fused_computation.7 | convolution fusion | flops 2684354560 | bytes 10747904 | tf_op jit(solution)/shard_map/dot_general | solution.py:609
  214.3 0.1 dynamic-slice_convert_fusion
  214.3 1.2 convolution_add_fusion.1
  215.6 1.5 fusion.3
  217.1 1.4 select_reduce_fusion
  218.5 0.5 slice_reduce_fusion.1
  (20 shorter events, 0.1 us)
Async XLA Ops:
  0.6 5.3 %copy-start.2 = (bf16[320,2048]{1,0:T(8,128)(2,1)S(1)}, bf16[320,2048]{1,0:T(8,128)(2,1)}, u32[]{:S(2)}) copy-start(bf16[320,2048]{1,0:T(8,128)(2,1)} %param.10) | copy-start | bytes 3932164
  6.0 2.3 %copy-start.3 = (bf16[320,2048]{1,0:T(8,128)(2,1)S(1)}, bf16[320,2048]{1,0:T(8,128)(2,1)}, u32[]{:S(2)}) copy-start(bf16[320,2048]{1,0:T(8,128)(2,1)} %param.11) | copy-start | bytes 3932164
  8.3 2.7 %copy-start.6 = (bf16[320,2]{0,1:T(2,128)(2,1)S(1)}, bf16[320,2]{0,1:T(2,128)(2,1)}, u32[]{:S(2)}) copy-start(bf16[320,2]{0,1:T(2,128)(2,1)} %param.13) | copy-start | bytes 3844
  129.5 1.8 copy-start.10
  131.4 0.7 copy-start.5
  136.2 2.7 %copy-start.4 = (bf16[320,2048]{1,0:T(8,128)(2,1)S(1)}, bf16[320,2048]{1,0:T(8,128)(2,1)}, u32[]{:S(2)}) copy-start(bf16[320,2048]{1,0:T(8,128)(2,1)} %fusion) | copy-start | bytes 3932164
  138.9 2.1 copy-start.1
  141.0 2.5 %copy-start = (bf16[8,160,2048]{2,1,0:T(8,128)(2,1)S(1)}, bf16[8,160,2048]{2,1,0:T(8,128)(2,1)}, u32[]{:S(2)}) copy-start(bf16[8,160,2048]{2,1,0:T(8,128)(2,1)} %get-tuple-element.24.part) | copy-start | bytes 15728644
  143.5 54.5 %copy-start.9 = (bf16[8,160,512]{2,1,0:T(8,128)(2,1)S(1)}, bf16[8,160,512]{2,1,0:T(8,128)(2,1)}, u32[]{:S(2)}) copy-start(bf16[8,160,512]{2,1,0:T(8,128)(2,1)} %get-tuple-element.31) | copy-start | bytes 3932164
  197.3 8.1 %slice-start = ((s8[5242880]{0:T(1024)(128)(4,1)}), s8[4194304]{0:T(1024)(128)(4,1)S(1)}, s32[]{:S(2)}) async-start(s8[5242880]{0:T(1024)(128)(4,1)} %bitcast.66), calls=%async_computation | async-start | bytes 8388608
  198.0 7.3 %slice-start.1 = ((s8[5242880]{0:T(1024)(128)(4,1)}), s8[1048576]{0:T(1024)(128)(4,1)S(1)}, s32[]{:S(2)}) async-start(s8[5242880]{0:T(1024)(128)(4,1)} %bitcast.66), calls=%async_computation.1 | async-start | bytes 2097152
  198.0 7.3 %copy-start.8 = (bf16[8,160,512]{2,1,0:T(8,128)(2,1)S(1)}, bf16[8,160,512]{2,1,0:T(8,128)(2,1)}, u32[]{:S(2)}) copy-start(bf16[8,160,512]{2,1,0:T(8,128)(2,1)} %get-tuple-element.30) | copy-start | bytes 3932164
  205.4 4.5 %copy-start.7 = (bf16[8,160,512]{2,1,0:T(8,128)(2,1)S(1)}, bf16[8,160,512]{2,1,0:T(8,128)(2,1)}, u32[]{:S(2)}) copy-start(bf16[8,160,512]{2,1,0:T(8,128)(2,1)} %get-tuple-element.29) | copy-start | bytes 3932164
